TPU v7x, 32 devices: a whole 2x2x4 slice. The times are simulated.
32 devices in a mesh: ep: 16 (over z, y, x), tp: 2 (over core).
Axes of the slice: x: 2, y: 2, z: 4, core: 2. Of those that a mesh axis runs over, the one named last changes fastest.
Arguments:
- tokens: bfloat16 [256, 2048], P('ep'), may hold values from -6 to 6
- norm_gain: float32 [2048], replicated, may hold values from 0.1 to 1.9
- query_weight: bfloat16 [2048, 1024], P('ep', 'tp'), may hold values from -0.125 to 0.125
- key_weight: bfloat16 [2048, 1024], P('ep', 'tp'), may hold values from -0.125 to 0.125
- value_weight: bfloat16 [2048, 1024], P('ep', 'tp'), may hold values from -0.125 to 0.125
- outgate_weight: bfloat16 [2048, 1024], P('ep', 'tp'), may hold values from -0.125 to 0.125
- input_weight: bfloat16 [2048, 8], P('ep', 'tp'), may hold values from -0.125 to 0.125
- forget_weight: bfloat16 [2048, 8], P('ep', 'tp'), may hold values from -0.125 to 0.125
- forget_bias: float32 [8], P('tp'), may hold values from -1 to 5
- memory: float32 [256, 8, 128, 128], P('ep', 'tp'), may hold values from -2.4 to 2.4
- stabilizer: float32 [256, 8], P('ep', 'tp'), may hold values from -3 to 3
- head_gain: float32 [1024], P('tp'), may hold values from 0.1 to 1.9
- mix_weight: bfloat16 [1024, 2048], P('tp', 'ep'), may hold values from -0.1875 to 0.1875
- second_gain: float32 [2048], replicated, may hold values from 0.1 to 1.9
- route_experts: int32 [256, 4], P('ep'), may hold values from 0 to 15, all different within a row; in each aligned block of 16 rows (0 to 15, 16 to 31, ...) at most 8 rows name the same one
- route_weight: float32 [256, 4], P('ep'), may hold values from 0.1 to 1
- expert_gate: bfloat16 [16, 2048, 2048], P('ep', None, 'tp'), may hold values from -0.5 to 0.5
- expert_up: bfloat16 [16, 2048, 2048], P('ep', None, 'tp'), may hold values from -0.5 to 0.5
- expert_down: bfloat16 [16, 2048, 2048], P('ep', 'tp'), may hold values from -0.03125 to 0.03125
- dense_gate: bfloat16 [4096, 2048], P(('ep', 'tp')), may hold values from -0.125 to 0.125
- dense_up: bfloat16 [4096, 2048], P(('ep', 'tp')), may hold values from -0.125 to 0.125
- dense_down: bfloat16 [4096, 2048], P(('ep', 'tp')), may hold values from -0.09375 to 0.09375
- branch_scale: float32 [2048], replicated, may hold values from 0.3 to 1.5
Outputs:
- mixed: bfloat16 [256, 2048], P('ep', 'tp')
- memory_new: float32 [256, 8, 128, 128], P('ep', 'tp')
- stabilizer_new: float32 [256, 8], P('ep', 'tp')
Inputs may be any that keep to these rules, and one draw needn't show every extreme that they name: `route_experts`: each row names 4 different experts. Within each aligned block of 16 rows no expert is named by more than 8 rows, and in every draw some expert is named by exactly 8 rows of some block.
All inputs are finite; a program needn't handle non-finite values.
Results may differ from a plain program's by a relative error of at most 0.03.
Values may be sent and summed in bfloat16 or wider, within the bound.
A program may use at most 128 MiB of HBM per device.

v0:
```python
import functools

import jax
import jax.numpy as jnp
from jax import lax
from jax.experimental import pallas as pl
from jax.experimental.pallas import tpu as pltpu
from jax.sharding import PartitionSpec as P

norm_eps = 1e-05
clamp_limit = 7.0
sigmoid_slope = 1.702


def rms_scale(values, gain):
    mean_square = jnp.mean(values * values, axis=-1, keepdims=True)
    return values * lax.rsqrt(mean_square + norm_eps) * gain


def clamped_unit(gate_pre, up_pre):
    gate_clamped = jnp.minimum(gate_pre, clamp_limit)
    up_clamped = jnp.clip(up_pre, -clamp_limit, clamp_limit)
    return (
        (up_clamped + 1.0) * gate_clamped * jax.nn.sigmoid(sigmoid_slope * gate_clamped)
    ).astype(jnp.bfloat16)


def memory_step(projected, forget_bias, memory, stabilizer, head_gain):
    query_rows, key_rows, value_rows, outgate_rows, input_pre, forget_pre = projected
    sequences, head_count = stabilizer.shape
    head_size = memory.shape[-1]
    log_forget = jax.nn.log_sigmoid(forget_pre + forget_bias)
    stab_new = jnp.maximum(log_forget + stabilizer, input_pre)
    carried = jnp.exp(log_forget + stabilizer - stab_new)
    written = jnp.exp(input_pre - stab_new)
    query_heads = query_rows.astype(jnp.float32).reshape(sequences, head_count, head_size)
    key_heads = key_rows.astype(jnp.float32).reshape(
        sequences, head_count, head_size
    ) * head_size ** (-0.5)
    value_heads = value_rows.astype(jnp.float32).reshape(sequences, head_count, head_size)
    memory_new = (
        carried[:, :, None, None] * memory
        + written[:, :, None, None] * value_heads[:, :, :, None] * key_heads[:, :, None, :]
    )
    readout = jnp.einsum("bhvk,bhk->bhv", memory_new, query_heads, precision=lax.Precision.HIGHEST)
    out_gate = jax.nn.sigmoid(
        outgate_rows.astype(jnp.float32).reshape(sequences, head_count, head_size)
    )
    gated = (rms_scale(readout, head_gain.reshape(head_count, head_size)) * out_gate).astype(
        jnp.bfloat16
    )
    return (gated.reshape(sequences, head_count * head_size), memory_new, stab_new)


def meet(count, me):
    barrier = pltpu.get_barrier_semaphore()

    def greet(step, carry):
        pl.semaphore_signal(
            barrier,
            inc=1,
            device_id={"ep": lax.rem(me + step, count)},
            device_id_type=pl.DeviceIdType.MESH,
        )
        return carry

    lax.fori_loop(1, count, greet, 0)
    pl.semaphore_wait(barrier, count - 1)


def link(count, me, step, source, landing, send_sem, recv_sem, gather):
    peer = lax.rem(me + step, count)
    return pltpu.make_async_remote_copy(
        src_ref=source if gather else source.at[peer],
        dst_ref=landing.at[me],
        send_sem=send_sem.at[step],
        recv_sem=recv_sem.at[step],
        device_id={"ep": peer},
        device_id_type=pl.DeviceIdType.MESH,
    )


def exchange_kernel(count, gather, source, landing, send_sem, recv_sem):
    me = lax.axis_index("ep")
    meet(count, me)

    def start(step, carry):
        link(count, me, step, source, landing, send_sem, recv_sem, gather).start()
        return carry

    def finish(step, carry):
        link(count, me, step, source, landing, send_sem, recv_sem, gather).wait()
        return carry

    lax.fori_loop(1, count, start, 0)
    landing[me] = source[...] if gather else source[me]
    lax.fori_loop(1, count, finish, 0)


def sum_kernel(count, source, total, landing, send_sem, recv_sem):
    me = lax.axis_index("ep")
    meet(count, me)

    def start(step, carry):
        link(count, me, step, source, landing, send_sem, recv_sem, False).start()
        return carry

    def finish(step, carry):
        link(count, me, step, source, landing, send_sem, recv_sem, False).wait()
        total[...] += landing[lax.rem(me + count - step, count)].astype(jnp.float32)
        return carry

    lax.fori_loop(1, count, start, 0)
    total[...] = source[me].astype(jnp.float32)
    lax.fori_loop(1, count, finish, 0)


def semaphores(count):
    return [pltpu.SemaphoreType.DMA((count,)), pltpu.SemaphoreType.DMA((count,))]


def in_vmem():
    return pl.BlockSpec(memory_space=pltpu.VMEM)


def exchange(blocks, count, name, gather=False):
    shape = (count,) + blocks.shape if gather else blocks.shape
    return pl.pallas_call(
        functools.partial(exchange_kernel, count, gather),
        out_shape=jax.ShapeDtypeStruct(shape, blocks.dtype),
        in_specs=[in_vmem()],
        out_specs=in_vmem(),
        scratch_shapes=semaphores(count),
        compiler_params=pltpu.CompilerParams(
            collective_id=name, has_side_effects=True, vmem_limit_bytes=16 * 2**20
        ),
    )(blocks)


def exchange_sum(blocks, count, name):
    return pl.pallas_call(
        functools.partial(sum_kernel, count),
        out_shape=jax.ShapeDtypeStruct(blocks.shape[1:], jnp.float32),
        in_specs=[in_vmem()],
        out_specs=in_vmem(),
        scratch_shapes=[pltpu.VMEM(blocks.shape, blocks.dtype)] + semaphores(count),
        compiler_params=pltpu.CompilerParams(
            collective_id=name, has_side_effects=True, vmem_limit_bytes=24 * 2**20
        ),
    )(blocks)


def split_parts(values, number):
    parts = []
    for _ in range(number):
        part = lax.reduce_precision(values, 8, 7)
        parts.append(part.astype(jnp.bfloat16))
        values = values - part
    return parts


def body(
    tokens,
    norm_gain,
    query_weight,
    key_weight,
    value_weight,
    outgate_weight,
    input_weight,
    forget_weight,
    forget_bias,
    memory,
    stabilizer,
    head_gain,
    mix_weight,
    second_gain,
    route_experts,
    route_weight,
    expert_gate,
    expert_up,
    expert_down,
    dense_gate,
    dense_up,
    dense_down,
    branch_scale,
):
    sequences, model_width = tokens.shape
    ep_count = lax.axis_size("ep")
    tp_count = lax.axis_size("tp")
    me, side = lax.axis_index("ep"), lax.axis_index("tp")
    swap = [(i, tp_count - 1 - i) for i in range(tp_count)]
    rows = sequences * ep_count
    part_width = model_width // tp_count
    own_width = model_width // ep_count
    lanes = 128
    first = side == 0

    inputs_float = tokens.astype(jnp.float32)
    normed = rms_scale(inputs_float, norm_gain).astype(jnp.bfloat16)
    matched = route_experts[:, :, None] == jnp.arange(ep_count)[None, None, :]
    weights = jnp.sum(jnp.where(matched, route_weight[:, :, None], 0.0), axis=1)
    weight_parts = jnp.stack(split_parts(weights, 3), axis=-1)
    weight_parts = jnp.pad(weight_parts, ((0, 0), (0, 0), (0, lanes - 3)))
    payload = jnp.concatenate(
        [
            normed.reshape(sequences, ep_count, own_width),
            tokens.reshape(sequences, ep_count, own_width),
            weight_parts,
        ],
        axis=2,
    ).transpose(1, 0, 2)
    columns = exchange(payload, ep_count, 1).reshape(rows, -1)
    token_columns = columns[:, own_width : 2 * own_width]
    row_weight = jnp.sum(
        columns[:, 2 * own_width : 2 * own_width + 3].astype(jnp.float32), axis=1, keepdims=True
    )

    wide = jnp.concatenate((query_weight, key_weight, value_weight, outgate_weight), axis=1)
    thin = jnp.concatenate((input_weight, forget_weight), axis=1)
    own_columns = columns[:, :own_width]
    wide_sums = jnp.dot(own_columns, wide, preferred_element_type=jnp.float32)
    thin_sums = jnp.dot(own_columns, thin, preferred_element_type=jnp.float32)
    gates = thin.shape[1]
    upper, under = split_parts(thin_sums, 2)
    partials = jnp.concatenate(
        [
            wide_sums.astype(jnp.bfloat16),
            jnp.pad(jnp.concatenate([upper, under], axis=1), ((0, 0), (0, lanes - 2 * gates))),
        ],
        axis=1,
    )
    sums = exchange_sum(partials.reshape(ep_count, sequences, -1), ep_count, 2)
    width = query_weight.shape[1]
    gate_sums = sums[:, 4 * width : 4 * width + gates] + sums[:, 4 * width + gates : 4 * width + 2 * gates]
    projected = tuple(
        sums[:, i * width : (i + 1) * width].astype(jnp.bfloat16) for i in range(4)
    ) + (gate_sums[:, : gates // 2], gate_sums[:, gates // 2 :])
    gated, memory_new, stab_new = memory_step(projected, forget_bias, memory, stabilizer, head_gain)

    all_gated = exchange(gated, ep_count, 3, gather=True).reshape(rows, -1)
    partial_value = jnp.dot(
        all_gated, mix_weight, preferred_element_type=jnp.float32
    ).astype(jnp.bfloat16)
    half = rows // tp_count
    upper, under = partial_value[:half], partial_value[half:]
    kept = jnp.where(first, upper, under)
    came = lax.ppermute(jnp.where(first, under, upper), "tp", swap)
    attended = kept.astype(jnp.float32) + came.astype(jnp.float32)
    token_half = jnp.where(first, token_columns[:half], token_columns[half:])
    residual_part = (token_half.astype(jnp.float32) + attended).astype(jnp.bfloat16)
    half_rows = exchange(residual_part, ep_count, 4, gather=True)
    half_rows = half_rows.transpose(1, 0, 2).reshape(half, model_width)
    other_rows = lax.ppermute(half_rows, "tp", swap)
    residual = jnp.concatenate(
        [jnp.where(first, half_rows, other_rows), jnp.where(first, other_rows, half_rows)], axis=0
    )
    normed_second = rms_scale(residual.astype(jnp.float32), second_gain).astype(jnp.bfloat16)

    gate_pre = jnp.dot(normed_second, expert_gate[0], preferred_element_type=jnp.float32)
    up_pre = jnp.dot(normed_second, expert_up[0], preferred_element_type=jnp.float32)
    expert_act = clamped_unit(gate_pre, up_pre)
    expert_out = jnp.dot(expert_act, expert_down[0], preferred_element_type=jnp.float32)
    gate_rows = jnp.einsum(
        "td,fd->tf", normed_second, dense_gate, preferred_element_type=jnp.float32
    )
    lift_rows = jnp.einsum("td,fd->tf", normed_second, dense_up, preferred_element_type=jnp.float32)
    dense_act = (jax.nn.silu(gate_rows) * lift_rows).astype(jnp.bfloat16)
    dense_out = jnp.dot(dense_act, dense_down, preferred_element_type=jnp.float32)
    term = dense_out * branch_scale + row_weight * expert_out
    left, right = term[:, :part_width], term[:, part_width:]
    passed = jnp.where(first, right, left).astype(jnp.bfloat16)
    received = lax.ppermute(passed, "tp", swap).astype(jnp.float32)
    summed = (jnp.where(first, left, right) + received).astype(jnp.bfloat16)
    branches = exchange_sum(summed.reshape(ep_count, sequences, part_width), ep_count, 5)
    own_residual = lax.dynamic_slice(
        residual, (me * sequences, side * part_width), (sequences, part_width)
    )
    mixed = own_residual.astype(jnp.float32) + branches
    return (mixed.astype(jnp.bfloat16), memory_new, stab_new)


def solution(mesh):
    in_specs = (
        P("ep", None),
        P(),
        P("ep", "tp"),
        P("ep", "tp"),
        P("ep", "tp"),
        P("ep", "tp"),
        P("ep", "tp"),
        P("ep", "tp"),
        P("tp"),
        P("ep", "tp", None, None),
        P("ep", "tp"),
        P("tp"),
        P("tp", "ep"),
        P(),
        P("ep", None),
        P("ep", None),
        P("ep", None, "tp"),
        P("ep", None, "tp"),
        P("ep", "tp", None),
        P(("ep", "tp"), None),
        P(("ep", "tp"), None),
        P(("ep", "tp"), None),
        P(),
    )
    out_specs = (P("ep", "tp"), P("ep", "tp", None, None), P("ep", "tp"))
    return jax.shard_map(body, mesh=mesh, in_specs=in_specs, out_specs=out_specs, check_vma=False)
```

profile of v0, /device:TPU:0, one launch (start us, length us, event | category | flops | bytes accessed | tf_op | source)
XLA Modules:
  0.0 117.1 jit_solution(17201675163299540545)
XLA Ops:
  0.6 0.0 copy-start
  0.6 0.8 select_reduce_fusion
  1.5 0.2 copy.53
  1.7 1.0 fusion.49
  2.7 1.0 copy_bitcast_fusion.1
  3.7 10.7 %shard_map.238 = bf16[16,16,384]{2,1,0:T(8,128)(2,1)S(1)} custom-call(bf16[16,16,384]{2,1,0:T(8,128)(2,1)S(1)} %fusion.48.source), custom_call_target="tpu_custom_call" | custom-call | tf_op jit(solution)/shard_map/pallas_call | solution.py:128
  14.4 0.8 reduce-precision_convert_fusion
  15.2 0.1 copy.56
  15.4 1.5 %convolution_convert_fusion = bf16[256,2048]{1,0:T(8,128)(2,1)S(1)} fusion(bf16[128,512]{1,0:T(8,128)(2,1)} %param.28, bf16[128,512]{1,0:T(8,128)(2,1)} %param.27, bf16[128,512]{1,0:T(8,128)(2,1)} %param.26, bf16[128,512]{1,0:T(8,128)(2,1)} %param.25, bf16[256,384]{1,0:T(8,128)(2,1)S(1)} %bitcast.78), kind=kOutput, calls=%fused_computation.12 | convolution fusion | flops 136839168 | bytes 1638400 | tf_op jit(solution)/shard_map/dot_general | solution.py:221
  16.9 0.0 copy-start.7
  16.9 0.0 copy-start.9
  16.9 0.1 fusion.32
  17.0 22.9 %shard_map.239 = f32[16,2176]{1,0:T(8,128)S(1)} custom-call(bf16[16,16,2176]{2,1,0:T(8,128)(2,1)S(1)} %bitcast.74), custom_call_target="tpu_custom_call" | custom-call | tf_op jit(solution)/shard_map/pallas_call | solution.py:141
  40.0 0.1 slice_add_fusion.1
  40.1 0.0 copy-done.7
  40.1 0.1 copy.57
  40.2 0.0 copy-done.9
  40.2 0.1 subtract_exponential_fusion.1
  40.3 0.1 broadcast_multiply_fusion
  40.4 3.0 %multiply_add_fusion = f32[16,4,128,128]{3,2,1,0:T(8,128)S(1)} fusion(f32[16,4,128,128]{3,2,1,0:T(8,128)} %param.32, f32[16,4,128]{2,1,0:T(4,128)S(1)} %mul.162, f32[16,4,128]{2,1,0:T(4,128)S(1)} %broadcast_multiply_fusion, f32[16,4]{1,0:T(8,128)S(1)} %get-tuple-element.15), kind=kLoop, calls=%fused_computation.6 | loop fusion | flops 3145728 | bytes 8454400 | tf_op jit(solution)/shard_map/add | solution.py:42
  43.5 0.0 copy-start.1
  43.5 0.0 copy-start.8
  43.5 0.0 copy-start.4
  43.5 3.3 %fusion.85 = f32[16,4,1,128]{3,2,1,0:T(1,128)S(1)} fusion(f32[16,4,128,128]{3,2,1,0:T(8,128)S(1)} %multiply_add_fusion, bf16[16,4,128,1]{2,3,1,0:T(2,128)(2,1)S(1)} %reshape.141), kind=kOutput, calls=%fused_computation.114 | convolution fusion | flops 12582912 | bytes 4243456 | tf_op jit(solution)/shard_map/bhvk,bhk->bhv/dot_general | solution.py:45
  46.8 0.0 copy-done.1
  46.8 0.1 multiply_reduce_fusion
  47.0 0.0 copy-done.8
  47.0 0.1 multiply_convert_fusion.2
  47.1 15.1 %shard_map.240 = bf16[16,16,512]{2,1,0:T(8,128)(2,1)S(1)} custom-call(bf16[16,512]{1,0:T(8,128)(2,1)S(1)} %bitcast.81), custom_call_target="tpu_custom_call" | custom-call | tf_op jit(solution)/shard_map/pallas_call | solution.py:128
  62.2 0.0 copy-done.4
  62.2 0.2 convolution_convert_fusion.1
  62.5 0.1 collective-permute-start
  62.5 1.2 %collective-permute-done = bf16[128,128]{1,0:T(8,128)(2,1)S(1)} collective-permute-done((bf16[128,128]{1,0:T(8,128)(2,1)S(1)}, bf16[128,128]{1,0:T(8,128)(2,1)S(1)}, u32[]{:S(2)}, u32[]{:S(2)}) %collective-permute-start) | collective-permute-done | bytes 32800 | tf_op jit(solution)/shard_map/ppermute | solution.py:247
  63.8 14.7 %shard_map.241 = bf16[16,128,128]{2,1,0:T(8,128)(2,1)S(1)} custom-call(bf16[128,128]{1,0:T(8,128)(2,1)S(1)} %add_convert_fusion.2.source), custom_call_target="tpu_custom_call" | custom-call | tf_op jit(solution)/shard_map/pallas_call | solution.py:128
  78.5 0.0 copy-start.5
  78.5 0.0 copy-start.10
  78.5 0.1 copy_bitcast_fusion
  78.6 0.1 collective-permute-start.1
  78.7 0.1 convert_reduce_fusion
  78.8 1.8 %collective-permute-done.1 = bf16[128,2048]{1,0:T(8,128)(2,1)S(1)} collective-permute-done((bf16[128,2048]{1,0:T(8,128)(2,1)S(1)}, bf16[128,2048]{1,0:T(8,128)(2,1)S(1)}, u32[]{:S(2)}, u32[]{:S(2)}) %collective-permute-start.1) | collective-permute-done | bytes 524320 | tf_op jit(solution)/shard_map/ppermute | solution.py:253
  80.6 0.2 broadcast_select_fusion.1
  80.8 0.0 copy-start.2
  80.8 0.3 fusion.11
  81.1 0.0 copy-done.5
  81.1 0.0 copy-done.10
  81.1 0.0 copy-start.11
  81.1 2.3 %fusion.14 = f32[256,1024]{1,0:T(8,128)} fusion(bf16[1,2048,1024]{2,1,0:T(8,128)(2,1)S(1)} %copy-done.10, f32[2048]{0:T(1024)S(1)} %copy-done.5, f32[256]{0:T(256)S(1)} %add_rsqrt_fusion.1, bf16[128,2048]{1,0:T(8,128)(2,1)S(1)} %get-tuple-element.18, bf16[128,2048]{1,0:T(8,128)(2,1)S(1)} %get-tuple-element.17), kind=kOutput, calls=%fused_computation.18 | convolution fusion | flops 1077673984 | bytes 6300672 | tf_op jit(solution)/shard_map/dot_general | solution.py:259
  83.4 0.0 copy-done.11
  83.4 0.5 fusion.82
  83.9 0.0 copy-done.2
  83.9 0.0 copy-start.6
  84.0 7.7 %fusion.6 = f32[256,2048]{1,0:T(8,128)} fusion(bf16[1,1024,2048]{2,1,0:T(8,128)(2,1)} %param.41, f32[256]{0:T(256)S(1)} %convert_reduce_fusion, f32[256,1024]{1,0:T(8,128)} %fusion.14, bf16[1,2048,1024]{2,1,0:T(8,128)(2,1)} %param.40, f32[2048]{0:T(1024)S(1)} %copy-done.5, f32[256]{0:T(256)S(1)} %add_rsqrt_fusion.1, ...), kind=kOutput, calls=%fused_computation.7 | convolution fusion | flops 2154037248 | bytes 12593152 | tf_op jit(solution)/shard_map/dot_general | solution.py:262
  91.6 0.0 copy-done
  91.6 0.0 copy-done.6
  91.6 3.2 %fusion.9 = f32[256,2048]{1,0:T(8,128)S(1)} fusion(f32[256,2048]{1,0:T(8,128)} %fusion.6, bf16[128,2048]{1,0:T(8,128)(2,1)S(1)} %copy-done, f32[2048]{0:T(1024)S(1)} %copy-done.6, f32[256,128]{1,0:T(8,128)S(1)} %fusion.82, bf16[128,2048]{1,0:T(8,128)(2,1)} %param.43, f32[2048]{0:T(1024)S(1)} %copy-done.5, f32[256]{0:T(256)S(1)} %add_rsqrt_fusion.1, ...), kind=kOutput, calls=%fused_computation.9 | convolution fusion | flops 273350656 | bytes 6439936 | tf_op jit(solution)/shard_map/dot_general | solution.py:268
  94.9 0.9 select_convert_fusion
  95.8 0.1 collective-permute-start.2
  95.9 0.7 copy.59
  96.6 0.0 copy-start.3
  96.6 1.5 %collective-permute-done.2 = bf16[256,1024]{1,0:T(8,128)(2,1)} collective-permute-done((bf16[256,1024]{1,0:T(8,128)(2,1)}, bf16[256,1024]{1,0:T(8,128)(2,1)}, u32[]{:S(2)}, u32[]{:S(2)}) %collective-permute-start.2) | collective-permute-done | bytes 524320 | tf_op jit(solution)/shard_map/ppermute | solution.py:272
  98.0 1.3 %add_convert_fusion = bf16[256,1024]{1,0:T(8,128)(2,1)S(1)} fusion(bf16[256,1024]{1,0:T(8,128)(2,1)} %collective-permute-done.2, f32[256,2048]{1,0:T(8,128)S(1)} %fusion.9, pred[]{:T(512)S(6)} %eq.16), kind=kLoop, calls=%fused_computation.29 | loop fusion | flops 1048576 | bytes 3145729 | tf_op jit(solution)/shard_map/convert_element_type | solution.py:273
  99.4 17.0 %shard_map.242 = f32[16,1024]{1,0:T(8,128)S(1)} custom-call(bf16[16,16,1024]{2,1,0:T(8,128)(2,1)S(1)} %bitcast.75), custom_call_target="tpu_custom_call" | custom-call | tf_op jit(solution)/shard_map/pallas_call | solution.py:141
  116.4 0.0 copy-done.3
  116.4 0.7 add_convert_fusion.1
  (18 shorter events, 0.2 us)
Async XLA Ops:
  0.6 91.0 %copy-start = (bf16[128,2048]{1,0:T(8,128)(2,1)S(1)}, bf16[128,2048]{1,0:T(8,128)(2,1)}, u32[]{:S(2)}) copy-start(bf16[128,2048]{1,0:T(8,128)(2,1)} %param.44) | copy-start | bytes 1572868
  16.9 23.2 %copy-start.7 = (f32[16,4]{0,1:T(4,128)S(1)}, f32[16,4]{0,1:T(4,128)}, u32[]{:S(2)}) copy-start(f32[16,4]{0,1:T(4,128)} %param.33) | copy-start | bytes 772
  16.9 23.3 %copy-start.9 = (f32[4]{0:T(128)S(1)}, f32[4]{0:T(128)}, u32[]{:S(2)}) copy-start(f32[4]{0:T(128)} %param.31) | copy-start | bytes 52
  43.5 3.4 %copy-start.1 = (f32[16,4,128,128]{3,2,1,0:T(8,128)}, f32[16,4,128,128]{3,2,1,0:T(8,128)S(1)}, u32[]{:S(2)}) copy-start(f32[16,4,128,128]{3,2,1,0:T(8,128)S(1)} %multiply_add_fusion) | copy-start | bytes 12582916
  43.5 3.5 %copy-start.8 = (f32[512]{0:T(512)S(1)}, f32[512]{0:T(512)}, u32[]{:S(2)}) copy-start(f32[512]{0:T(512)} %param.34) | copy-start | bytes 6148
  43.5 18.7 %copy-start.4 = (bf16[512,128]{1,0:T(8,128)(2,1)S(1)}, bf16[512,128]{1,0:T(8,128)(2,1)}, u32[]{:S(2)}) copy-start(bf16[512,128]{1,0:T(8,128)(2,1)} %param.35) | copy-start | bytes 393220
  62.5 1.3 %collective-permute-start = (bf16[128,128]{1,0:T(8,128)(2,1)S(1)}, bf16[128,128]{1,0:T(8,128)(2,1)S(1)}, u32[]{:S(2)}, u32[]{:S(2)}) collective-permute-start(bf16[128,128]{1,0:T(8,128)(2,1)S(1)} %broadcast_select_fusion.2), channel_id=1, source_target_pairs={{0,1},{1,0},{2,3},{3,2},{4,5},{5,4},{6,7},{7,6},{8,9},{9,8},{10,11... | collective-permute-start | bytes 98312 | tf_op jit(solution)/shard_map/ppermute | solution.py:247
  78.5 2.6 %copy-start.5 = (f32[2048]{0:T(1024)S(1)}, f32[2048]{0:T(1024)}, u32[]{:S(2)}) copy-start(f32[2048]{0:T(1024)} %param.36) | copy-start | bytes 24580
  78.5 2.6 %copy-start.10 = (bf16[1,2048,1024]{2,1,0:T(8,128)(2,1)S(1)}, bf16[1,2048,1024]{2,1,0:T(8,128)(2,1)}, u32[]{:S(2)}) copy-start(bf16[1,2048,1024]{2,1,0:T(8,128)(2,1)} %param.39) | copy-start | bytes 12582916
  78.6 2.0 %collective-permute-start.1 = (bf16[128,2048]{1,0:T(8,128)(2,1)S(1)}, bf16[128,2048]{1,0:T(8,128)(2,1)S(1)}, u32[]{:S(2)}, u32[]{:S(2)}) collective-permute-start(bf16[128,2048]{1,0:T(8,128)(2,1)S(1)} %copy_bitcast_fusion), channel_id=1, source_target_pairs={{0,1},{1,0},{2,3},{3,2},{4,5},{5,4},{6,7},{7,6},{8,9},{9,8},{10,11... | collective-permute-start | bytes 1572872 | tf_op jit(solution)/shard_map/ppermute | solution.py:253
  80.8 3.2 %copy-start.2 = (bf16[128,2048]{1,0:T(8,128)(2,1)}, bf16[128,2048]{1,0:T(8,128)(2,1)S(1)}, u32[]{:S(2)}) copy-start(bf16[128,2048]{1,0:T(8,128)(2,1)S(1)} %get-tuple-element.18) | copy-start | bytes 1572868
  81.1 2.4 %copy-start.11 = (bf16[128,2048]{1,0:T(8,128)(2,1)S(1)}, bf16[128,2048]{1,0:T(8,128)(2,1)}, u32[]{:S(2)}) copy-start(bf16[128,2048]{1,0:T(8,128)(2,1)} %param.42) | copy-start | bytes 1572868
  83.9 7.7 %copy-start.6 = (f32[2048]{0:T(1024)S(1)}, f32[2048]{0:T(1024)}, u32[]{:S(2)}) copy-start(f32[2048]{0:T(1024)} %param.45) | copy-start | bytes 24580
  95.8 2.3 %collective-permute-start.2 = (bf16[256,1024]{1,0:T(8,128)(2,1)}, bf16[256,1024]{1,0:T(8,128)(2,1)}, u32[]{:S(2)}, u32[]{:S(2)}) collective-permute-start(bf16[256,1024]{1,0:T(8,128)(2,1)} %select_convert_fusion), channel_id=1, source_target_pairs={{0,1},{1,0},{2,3},{3,2},{4,5},{5,4},{6,7},{7,6},{8,9},{9,8},{10,11... | collective-permute-start | bytes 1572872 | tf_op jit(solution)/shard_map/ppermute | solution.py:272
  96.6 19.8 %copy-start.3 = (bf16[128,2048]{1,0:T(8,128)(2,1)S(1)}, bf16[128,2048]{1,0:T(8,128)(2,1)}, u32[]{:S(2)}) copy-start(bf16[128,2048]{1,0:T(8,128)(2,1)} %copy-done.2) | copy-start | bytes 1572868
where the time goes:
time: 119 us; the launch traced here: 117 us
  Pallas kernels  80.4 us (68%)
  matrix products  19.7 us (17%)
  other arithmetic  9.97 us (8%)
  waiting for transfers between devices  4.44 us (4%)
  local copies, waits for them, and re-layouts  1.28 us (1%)
    pallas_call x3, Pallas kernels, exchange(): pl.pallas_call(functools.partial(exchange_kernel, count, gather), out_sha...  40.5 us
    pallas_call x2, Pallas kernels, exchange_sum(): pl.pallas_call(functools.partial(sum_kernel, count), out_shape=jax.ShapeD...  39.9 us
    dot_general x1, matrix products, body(): jnp.dot(expert_act, expert_down[0], preferred_element_type=jnp.float32)  7.68 us
    dot_general x1, matrix products, memory_step(): jnp.einsum('bhvk,bhk->bhv', memory_new, query_heads, precision=lax.Precis...  3.35 us
    dot_general x1, matrix products, body(): jnp.dot(dense_act, dense_down, preferred_element_type=jnp.float32)  3.25 us
    add x1, other arithmetic, memory_step(): carried[:, :, None, None] * memory  3.04 us
  transfers between devices with their start and end apart: 3, of which 3 were waited for; matrix products, arithmetic and copies ran while one was open for 1% of the time, Pallas kernels for 0%

commit v1 on v0

v1 whole, which is shorter than its diff:
```python
import functools

import jax
import jax.numpy as jnp
from jax import lax
from jax.experimental import pallas as pl
from jax.experimental.pallas import tpu as pltpu
from jax.sharding import PartitionSpec as P

norm_eps = 1e-05
clamp_limit = 7.0
sigmoid_slope = 1.702
lanes = 128
f32 = jnp.float32
bf16 = jnp.bfloat16


def loop(lower, upper, step):
    def run(index, carry):
        step(index)
        return carry

    lax.fori_loop(lower, upper, run, 0)


def remote(source, landing, send_sem, recv_sem, **target):
    return pltpu.make_async_remote_copy(
        src_ref=source,
        dst_ref=landing,
        send_sem=send_sem,
        recv_sem=recv_sem,
        device_id=target,
        device_id_type=pl.DeviceIdType.MESH,
    )


def greet(barrier, **target):
    pl.semaphore_signal(
        barrier, inc=1, device_id=target, device_id_type=pl.DeviceIdType.MESH
    )


class Place:
    def __init__(self, outer, inner):
        self.outer, self.inner = outer, inner
        self.me = lax.axis_index("ep")
        self.side = lax.axis_index("tp")
        self.o = self.me // inner
        self.n = self.me % inner

    def plane(self, step):
        return (self.o + step) % self.outer

    def spot(self, step):
        return (self.n + step) % self.inner

    def at(self, plane, spot):
        return plane * self.inner + spot


def gather(place, slot, send_sem, recv_sem, arrived):
    outer, inner, me = place.outer, place.inner, place.me

    def copy(source, target):
        return remote(
            slot(source), slot(source), send_sem, recv_sem.at[source], ep=target
        )

    loop(1, outer, lambda t: copy(me, place.at(place.plane(t), place.n)).start())
    loop(1, inner, lambda u: copy(me, place.at(place.o, place.spot(u))).start())
    arrived(me)

    def relay(t):
        source = place.at(place.plane(t), place.n)
        copy(source, source).wait_recv()
        loop(
            1,
            inner,
            lambda u: copy(source, place.at(place.o, place.spot(u))).start(),
        )
        arrived(source)

    loop(1, outer, relay)

    def take(t):
        def one(u):
            source = place.at(place.plane(t), place.spot(u))
            copy(source, source).wait_recv()
            arrived(source)

        loop(1, inner, one)

    loop(0, outer, take)


def sigmoid(values):
    return 1.0 / (1.0 + jnp.exp(-values))


def first_kernel(
    outer,
    inner,
    tok_in,
    norm_gain_in,
    wq,
    wk,
    wv,
    wo,
    wi_in,
    wf_in,
    bias_in,
    stab_in,
    head_gain_in,
    mix_in,
    rexp_in,
    rwt_in,
    mem_in,
    res,
    rww,
    stab_out,
    mem,
    tok,
    norm_gain,
    wide,
    wi,
    wf,
    bias,
    stab,
    hgain,
    mix,
    rexp,
    rwt,
    nbuf,
    nland,
    tbuf,
    tland,
    rbuf,
    pg,
    gland1,
    gmid,
    gland2,
    pbuf,
    land1,
    mid,
    land2,
    mid_half,
    land2_half,
    turned,
    carried_rows,
    written_rows,
    gland,
    pv,
    came,
    in_s,
    wide_s,
    p1_s,
    p1_r,
    tk_s,
    tk_r,
    rt_s,
    rt_r,
    g1_s,
    g1_r,
    g2_s,
    g2_r,
    l1_s,
    l1_r,
    l2_s,
    l2_r,
    l3_s,
    l3_r,
    mi,
    ag_s,
    ag_r,
    ap_r,
    tp_s,
    tp_r,
    ar_s,
    ar_r,
    sb_s,
    sb_r,
):
    place = Place(outer, inner)
    me, side, o, n = place.me, place.side, place.o, place.n
    count = outer * inner
    sequences, heads, size = mem.shape[0], mem.shape[1], mem.shape[2]
    width = nland.shape[2]
    rows = count * sequences
    half = pv.shape[1]
    per_half = count // 2
    sibling = 1 - side

    barrier = pltpu.get_barrier_semaphore()
    loop(1, count, lambda t: greet(barrier, ep=(me + t) % count))
    greet(barrier, tp=sibling)
    small = [
        pltpu.make_async_copy(source, target, in_s.at[i])
        for i, (source, target) in enumerate(
            (
                (tok_in, tok),
                (norm_gain_in, norm_gain),
                (rexp_in, rexp),
                (rwt_in, rwt),
                (wi_in, wi),
                (wf_in, wf),
                (bias_in, bias),
                (stab_in, stab),
                (head_gain_in, hgain),
                (mix_in, mix),
            )
        )
    ]
    for copy in small[:6]:
        copy.start()

    def wide_copies(h):
        part = slice(h * size, (h + 1) * size)
        return [
            pltpu.make_async_copy(
                weight.at[:, part],
                wide.at[h, :, slice(j * size, (j + 1) * size)],
                wide_s.at[4 * h + j],
            )
            for j, weight in enumerate((wq, wk, wv, wo))
        ]

    for h in range(heads):
        for copy in wide_copies(h):
            copy.start()
    for copy in small[6:]:
        copy.start()
    loop(
        0,
        heads,
        lambda h: pltpu.make_async_copy(mem_in.at[:, h], mem.at[:, h], mi.at[h]).start(),
    )

    small[0].wait()
    small[1].wait()
    tokens = tok[...].astype(f32)
    mean_square = jnp.mean(tokens * tokens, axis=-1, keepdims=True)
    normed = (tokens * lax.rsqrt(mean_square + norm_eps) * norm_gain[...]).astype(bf16)
    for p in range(count):
        nbuf[p] = normed[:, p * width : (p + 1) * width]
        tbuf[p] = tok[:, p * width : (p + 1) * width]

    small[2].wait()
    small[3].wait()
    topk = rexp.shape[0]
    experts = lax.broadcasted_iota(jnp.int32, (count, sequences), 0)
    weights = jnp.zeros((count, sequences), f32)
    for k in range(topk):
        weights += jnp.where(rexp[k : k + 1, :] == experts, rwt[k : k + 1, :], 0.0)
    rbuf[...] = jnp.zeros_like(rbuf)
    for p in range(count):
        rbuf[p, :, :sequences] = weights[p : p + 1, :]

    with jax.named_scope("barrier"):
        pl.semaphore_wait(barrier, count)

    def send_normed(t):
        peer = (me + t) % count
        remote(nbuf.at[peer], nland.at[me], p1_s, p1_r, ep=peer).start()

    loop(1, count, send_normed)
    mine = side == me // per_half

    def token_copy(t):
        peer = (me + t) % count
        return remote(
            tbuf.at[peer], tland.at[me % per_half], tk_s, tk_r.at[me % per_half], ep=peer
        )

    @pl.when(mine)
    def _():
        loop(1, count, lambda t: token_copy(t).start())
        tland[me % per_half] = tbuf[me]

    def send_route(t):
        peer = (me + t) % count
        remote(rbuf.at[peer], rww.at[me], rt_s, rt_r, ep=peer).start()

    loop(1, count, send_route)
    rww[me] = rbuf[me]
    nland[me] = nbuf[me]

    small[4].wait()
    small[5].wait()
    gates = 2 * heads
    once = jnp.concatenate((wi[...].astype(f32), wf[...].astype(f32)), axis=0)
    thin = jnp.concatenate(
        (once, once, jnp.zeros((lanes - 2 * gates, width), f32)), axis=0
    ).astype(bf16)

    with jax.named_scope("normed"):
        others = nland.at[pl.ds(0, count - 1)]
        remote(others, others, p1_s, p1_r, ep=me).wait_recv()
    columns = nland[...].reshape(rows, width)

    lane = lax.broadcasted_iota(jnp.int32, (rows, lanes), 1)
    thin_sums = lax.dot_general(
        columns, thin, (((1,), (1,)), ((), ())), preferred_element_type=f32
    )
    upper = thin_sums.astype(bf16).astype(f32)
    parted = jnp.where(lane < gates, upper, thin_sums - upper).astype(bf16)
    pg[...] = parted.reshape(outer, inner, sequences, lanes)

    def send_gates(t):
        spot = place.spot(t)
        remote(
            pg.at[:, spot], gland1.at[n], g1_s, g1_r, ep=place.at(o, spot)
        ).start()

    loop(1, inner, send_gates)

    def send_part(h, plane):
        def send(t):
            spot = place.spot(t)
            remote(
                pbuf.at[h, plane, spot],
                land1.at[h, plane, n],
                l1_s,
                l1_r.at[h * outer + plane],
                ep=place.at(o, spot),
            ).start()

        loop(1, inner, send)

    for h in range(heads):
        for copy in wide_copies(h):
            copy.wait()
        sums = jnp.dot(columns, wide[h], preferred_element_type=f32).astype(bf16)
        pbuf[h] = sums.reshape(outer, inner, sequences, 4 * size)
        loop(1, outer, lambda t: send_part(h, place.plane(t)))
        if h > 0:
            send_part(h - 1, o)
    send_part(heads - 1, o)
    for copy in small[6:]:
        copy.wait()

    with jax.named_scope("gates"):
        others = gland1.at[pl.ds(0, inner - 1)]
        remote(others, others, g1_s, g1_r, ep=me).wait_recv()
    for a in range(outer):
        total = pg[a, n].astype(f32)
        for t in range(1, inner):
            total += gland1[place.spot(t), a].astype(f32)
        gmid[a] = total

    def pass_gates(t):
        plane = place.plane(t)
        remote(
            gmid.at[plane], gland2.at[o], g2_s, g2_r, ep=place.at(plane, n)
        ).start()

    loop(1, outer, pass_gates)

    def plane_sum(h, plane):
        with jax.named_scope("first"):
            others = land1.at[h, plane, pl.ds(0, inner - 1)]
            remote(others, others, l1_s, l1_r.at[h * outer + plane], ep=me).wait_recv()
        total = pbuf[h, plane, n].astype(f32)
        for t in range(1, inner):
            total += land1[h, plane, place.spot(t)].astype(f32)
        return total

    def first_sum(h):
        def send(t):
            plane = place.plane(t)
            total = plane_sum(h, plane)
            mid[h, plane] = total[:, : 2 * size]
            mid_half[h, plane] = total[:, 2 * size :].astype(bf16)
            target = place.at(plane, n)
            remote(mid.at[h, plane], land2.at[h, o], l2_s, l2_r.at[h], ep=target).start()
            remote(
                mid_half.at[h, plane], land2_half.at[h, o], l3_s, l3_r.at[h], ep=target
            ).start()

        loop(1, outer, send)

    def gate_math():
        with jax.named_scope("gates2"):
            others = gland2.at[pl.ds(0, outer - 1)]
            remote(others, others, g2_s, g2_r, ep=me).wait_recv()
        total = gmid[o]
        for t in range(1, outer):
            total += gland2[place.plane(t)]
        turn = jnp.transpose(total)
        turn = turn[:gates] + turn[gates : 2 * gates]
        input_pre, forget_pre = turn[:heads], turn[heads:]
        square = lax.broadcasted_iota(jnp.int32, (heads, heads), 0) == lax.broadcasted_iota(
            jnp.int32, (heads, heads), 1
        )
        shift = jnp.sum(jnp.where(square, bias[...], 0.0), axis=1, keepdims=True)
        shifted = forget_pre + shift
        log_forget = jnp.minimum(shifted, 0.0) - jnp.log1p(jnp.exp(-jnp.abs(shifted)))
        stab_new = jnp.maximum(log_forget + stab[...], input_pre)
        stab_out[...] = stab_new
        turned[...] = jnp.zeros_like(turned)
        turned[:heads, :sequences] = jnp.exp(log_forget + stab[...] - stab_new)
        turned[heads:gates, :sequences] = jnp.exp(input_pre - stab_new)
        back = jnp.transpose(turned[...])[:sequences]
        for h in range(heads):
            carried_rows[h] = jnp.broadcast_to(back[:, h : h + 1], (sequences, lanes))
            written_rows[h] = jnp.broadcast_to(
                back[:, heads + h : heads + h + 1], (sequences, lanes)
            )

    def memory_head(h):
        own = plane_sum(h, o)
        with jax.named_scope("heads"):
            others = land2.at[h, pl.ds(0, outer - 1)]
            remote(others, others, l2_s, l2_r.at[h], ep=me).wait_recv()
            others = land2_half.at[h, pl.ds(0, outer - 1)]
            remote(others, others, l3_s, l3_r.at[h], ep=me).wait_recv()
        pltpu.make_async_copy(mem_in.at[:, h], mem.at[:, h], mi.at[h]).wait()
        query_key, value_gate = own[:, : 2 * size], own[:, 2 * size :]
        for t in range(1, outer):
            query_key += land2[h, place.plane(t)]
            value_gate += land2_half[h, place.plane(t)].astype(f32)
        query_key = query_key.astype(bf16).astype(f32)
        value_gate = value_gate.astype(bf16).astype(f32)
        query = query_key[:, :size]
        key = query_key[:, size:] * size**-0.5 * written_rows[h]
        value = value_gate[:, :size]
        outgate = value_gate[:, size:]
        carry = carried_rows[h]
        value_columns = jnp.transpose(value)
        places = lax.broadcasted_iota(jnp.int32, (size, lanes), 1)
        readout_columns = jnp.zeros((size, lanes), f32)
        for s in range(sequences):
            updated = (
                carry[s : s + 1, :] * mem[s, h] + value_columns[:, s : s + 1] * key[s : s + 1, :]
            )
            mem[s, h] = updated
            column = jnp.sum(updated * query[s : s + 1, :], axis=1, keepdims=True)
            readout_columns = jnp.where(places == s, column, readout_columns)
        readout = jnp.transpose(readout_columns)[:sequences]
        mean_square = jnp.mean(readout * readout, axis=-1, keepdims=True)
        gated = (
            readout
            * lax.rsqrt(mean_square + norm_eps)
            * hgain[h : h + 1, :]
            * sigmoid(outgate)
        )
        gland[h, me] = gated.astype(bf16)
        block = gland.at[h, me]
        loop(
            1,
            outer,
            lambda t: remote(
                block, block, ag_s, ag_r.at[h], ep=place.at(place.plane(t), n)
            ).start(),
        )
        loop(
            1,
            inner,
            lambda u: remote(
                block, block, ag_s, ap_r.at[h], ep=place.at(o, place.spot(u))
            ).start(),
        )

    def relay(h):
        others = gland.at[h, pl.ds(0, outer - 1)]
        remote(others, others, ag_s, ag_r.at[h], ep=me).wait_recv()

        def one(t):
            block = gland.at[h, place.at(place.plane(t), n)]
            loop(
                1,
                inner,
                lambda u: remote(
                    block, block, ag_s, ap_r.at[h], ep=place.at(o, place.spot(u))
                ).start(),
            )

        loop(1, outer, one)

    first_sum(0)
    gate_math()

    def both(h):
        first_sum(h)
        memory_head(h - 1)

        if h > 1:
            relay(h - 2)

    for h in range(1, heads):
        both(h)
    memory_head(heads - 1)

    with jax.named_scope("gated"):
        if heads > 1:
            relay(heads - 2)
        relay(heads - 1)
        partial = jnp.zeros((rows, width), f32)
        for h in range(heads):
            others = gland.at[h, pl.ds(0, outer * (inner - 1))]
            remote(others, others, ag_s, ap_r.at[h], ep=me).wait_recv()
            partial += jnp.dot(
                gland[h].reshape(rows, size),
                mix[h * size : (h + 1) * size, :],
                preferred_element_type=f32,
            )
        partial = partial.astype(bf16)
    pv[...] = partial.reshape(2, half, width)
    swap = remote(pv.at[sibling], came, tp_s, tp_r, tp=sibling)
    swap.start()

    def take_tokens(b):
        source = side * per_half + b

        @pl.when(source != me)
        def _():
            remote(tland.at[b], tland.at[b], tk_s, tk_r.at[b], ep=source).wait_recv()

    loop(0, per_half, take_tokens)
    with jax.named_scope("swap"):
        swap.wait_recv()
    attended = pv[side].astype(f32) + came[...].astype(f32)
    residual = (tland[...].reshape(half, width).astype(f32) + attended).astype(bf16)
    if len(res.shape) == 3:
        res[side, :, pl.ds(pl.multiple_of(me * width, width), width)] = residual
    else:
        res[me, side] = residual

    def slot(p, core):
        if len(res.shape) == 3:
            return res.at[core, :, pl.ds(pl.multiple_of(p * width, width), width)]
        return res.at[p, core]

    def hand(p):
        remote(slot(p, side), slot(p, side), sb_s, sb_r, tp=sibling).start()

    with jax.named_scope("rows"):
        gather(place, lambda p: slot(p, side), ar_s, ar_r, hand)

    with jax.named_scope("settle"):
        if len(res.shape) == 3:
            whole, sent = res.at[sibling], res.at[side, :, pl.ds(0, (count - 1) * width)]
        else:
            whole, sent = res.at[:, sibling], res.at[pl.ds(0, count - 1), side]
        remote(whole, whole, sb_s, sb_r, tp=sibling).wait()

    remote(sent, sent, ar_s, ar_r.at[0], ep=me).wait_send()
    others = rww.at[pl.ds(0, count - 1)]
    remote(others, others, rt_s, rt_r, ep=me).wait()
    others = nbuf.at[pl.ds(0, count - 1)]
    remote(others, others, p1_s, p1_r, ep=me).wait_send()

    @pl.when(mine)
    def _():
        remote(others, others, tk_s, tk_r.at[0], ep=me).wait_send()

    others = gland1.at[pl.ds(0, inner - 1)]
    remote(others, others, g1_s, g1_r, ep=me).wait_send()
    others = gmid.at[pl.ds(0, outer - 1)]
    remote(others, others, g2_s, g2_r, ep=me).wait_send()
    others = pbuf.at[:, :, pl.ds(0, inner - 1)]
    remote(others, others, l1_s, l1_r.at[0], ep=me).wait_send()
    others = mid.at[:, pl.ds(0, outer - 1)]
    remote(others, others, l2_s, l2_r.at[0], ep=me).wait_send()
    others = mid_half.at[:, pl.ds(0, outer - 1)]
    remote(others, others, l3_s, l3_r.at[0], ep=me).wait_send()
    others = gland.at[:, pl.ds(0, count - 1)]
    remote(others, others, ag_s, ag_r.at[0], ep=me).wait_send()
    swap.wait_send()


def second_kernel(
    outer,
    inner,
    chunks,
    row_blocks,
    res,
    rww,
    gain_in,
    scale_in,
    wg,
    wu,
    wd,
    dg,
    du,
    dd,
    out,
    gain,
    scale,
    wgv,
    wuv,
    wdv,
    dgv,
    duv,
    ddv,
    normed,
    dense_act,
    row_weight,
    act,
    passed,
    landed,
    kept,
    summed,
    land1,
    mid,
    land2,
    wg_m,
    wu_m,
    wd_m,
    d_m,
    tp_s,
    tp_r,
    l1_s,
    l1_r,
    l2_s,
    l2_r,
):
    place = Place(outer, inner)
    me, side, o, n = place.me, place.side, place.o, place.n
    count = outer * inner
    rows, model_width = normed.shape
    sequences = rows // count
    sibling = 1 - side
    hidden_chunk = wgv.shape[2]
    column_chunk = wdv.shape[2]
    part_width = chunks * column_chunk

    barrier = pltpu.get_barrier_semaphore()
    loop(1, inner, lambda u: greet(barrier, ep=place.at(o, place.spot(u))))
    loop(1, outer, lambda t: greet(barrier, ep=place.at(place.plane(t), n)))
    greet(barrier, tp=sibling)

    dense = [
        pltpu.make_async_copy(source, target, d_m.at[i])
        for i, (source, target) in enumerate(
            ((dg, dgv), (du, duv), (dd, ddv), (gain_in, gain), (scale_in, scale))
        )
    ]
    hidden_chunks = wgv.shape[0]

    def gate_copy(c):
        span = pl.ds(c * hidden_chunk, hidden_chunk)
        return pltpu.make_async_copy(wg.at[0, :, span], wgv.at[c], wg_m.at[c])

    def up_copy(c):
        span = pl.ds(c * hidden_chunk, hidden_chunk)
        return pltpu.make_async_copy(wu.at[0, :, span], wuv.at[c], wu_m.at[c])

    def down_copy(c):
        span = pl.ds(c * column_chunk, column_chunk)
        return pltpu.make_async_copy(wd.at[0, :, span], wdv.at[c], wd_m.at[c])

    dense[3].start()
    dense[0].start()
    dense[1].start()
    for c in range(hidden_chunks):
        gate_copy(c).start()
        up_copy(c).start()
    dense[2].start()
    dense[4].start()
    for c in range(chunks):
        down_copy(sibling * chunks + c).start()
        down_copy(side * chunks + c).start()

    block = act.shape[0] // row_blocks

    def norm_rows(r):
        span = pl.ds(pl.multiple_of(r * norm_block, norm_block), norm_block)
        values = res[span, :].astype(f32)
        mean_square = jnp.mean(values * values, axis=-1, keepdims=True)
        normed[span, :] = (values * lax.rsqrt(mean_square + norm_eps) * gain[...]).astype(bf16)

    norm_block = min(rows, 32)
    dense[3].wait()
    with jax.named_scope("norm"):
        loop(0, rows // norm_block, norm_rows)
    received = jnp.broadcast_to(rww[...], (count, sequences, lanes)).reshape(rows, lanes)
    line = lax.broadcasted_iota(jnp.int32, (rows, lanes), 0) % sequences
    lane = lax.broadcasted_iota(jnp.int32, (rows, lanes), 1)
    row_weight[...] = jnp.sum(jnp.where(line == lane, received, 0.0), axis=-1, keepdims=True)

    against = (((1,), (1,)), ((), ()))
    dense[0].wait()
    dense[1].wait()

    def part(r):
        return pl.ds(pl.multiple_of(r * block, block), block)

    def dense_rows(r):
        gate_rows = lax.dot_general(
            normed[part(r), :], dgv[...], against, preferred_element_type=f32
        )
        lift_rows = lax.dot_general(
            normed[part(r), :], duv[...], against, preferred_element_type=f32
        )
        dense_act[part(r), :] = (gate_rows * sigmoid(gate_rows) * lift_rows).astype(bf16)

    with jax.named_scope("dense"):
        loop(0, row_blocks, dense_rows)

    def hidden_step(c):
        gate_copy(c).wait()
        up_copy(c).wait()

        def one(r):
            gate_pre = jnp.dot(normed[part(r), :], wgv[c], preferred_element_type=f32)
            up_pre = jnp.dot(normed[part(r), :], wuv[c], preferred_element_type=f32)
            gate_pre = jnp.minimum(gate_pre, clamp_limit)
            up_pre = jnp.clip(up_pre, -clamp_limit, clamp_limit)
            span = pl.ds(pl.multiple_of(c * hidden_chunk, hidden_chunk), hidden_chunk)
            act[part(r), span] = (
                (up_pre + 1.0) * gate_pre * sigmoid(sigmoid_slope * gate_pre)
            ).astype(bf16)

        loop(0, row_blocks, one)

    with jax.named_scope("hidden"):
        loop(0, hidden_chunks, hidden_step)

    dense[2].wait()
    dense[4].wait()
    pl.semaphore_wait(barrier, inner + outer - 1)

    def term(c, r):
        span = pl.ds(pl.multiple_of(c * column_chunk, column_chunk), column_chunk)
        routed = jnp.dot(act[part(r), :], wdv[c], preferred_element_type=f32)
        dense_out = jnp.dot(dense_act[part(r), :], ddv[:, span], preferred_element_type=f32)
        return dense_out * scale[:, span] + row_weight[part(r), :] * routed

    def cross(c):
        return remote(passed.at[c], landed.at[c], tp_s, tp_r.at[c], tp=sibling)

    def spread_plane(c, plane):
        def send(t):
            spot = place.spot(t)
            remote(
                summed.at[c, plane, spot],
                land1.at[c, plane, n],
                l1_s,
                l1_r.at[c * outer + plane],
                ep=place.at(o, spot),
            ).start()

        loop(1, inner, send)

    def spread(c):
        cross(c).wait_recv()
        both = kept[c] + landed[c].astype(f32)
        summed[c] = both.astype(bf16).reshape(outer, inner, sequences, column_chunk)

        loop(1, outer, lambda t: spread_plane(c, place.plane(t)))

    def give_step(c):
        down_copy(sibling * chunks + c).wait()

        def give(r):
            passed[c, part(r), :] = term(sibling * chunks + c, r).astype(bf16)

        loop(0, row_blocks, give)
        cross(c).start()

    def keep_step(c):
        down_copy(side * chunks + c).wait()

        def keep(r):
            kept[c, part(r), :] = term(side * chunks + c, r)

        loop(0, row_blocks, keep)
        spread(c)

    with jax.named_scope("give"):
        loop(0, chunks, give_step)
    with jax.named_scope("keep"):
        loop(0, chunks, keep_step)

    loop(0, chunks, lambda c: spread_plane(c, o))

    def plane_sum(c, plane):
        others = land1.at[c, plane, pl.ds(0, inner - 1)]
        remote(others, others, l1_s, l1_r.at[c * outer + plane], ep=me).wait_recv()
        total = summed[c, plane, n].astype(f32)
        for t in range(1, inner):
            total += land1[c, plane, place.spot(t)].astype(f32)
        return total

    def first_sum(c):
        def send(t):
            plane = place.plane(t)
            mid[c, plane] = plane_sum(c, plane).astype(bf16)
            remote(
                mid.at[c, plane], land2.at[c, o], l2_s, l2_r.at[c], ep=place.at(plane, n)
            ).start()

        loop(1, outer, send)

    with jax.named_scope("sum1"):
        loop(0, chunks, first_sum)

    residual = res[
        pl.ds(pl.multiple_of(me * sequences, sequences), sequences),
        pl.ds(pl.multiple_of(side * part_width, part_width), part_width),
    ].astype(f32)

    with jax.named_scope("sum2"):
        for c in range(chunks):
            total = plane_sum(c, o)
            others = land2.at[c, pl.ds(0, outer - 1)]
            remote(others, others, l2_s, l2_r.at[c], ep=me).wait_recv()
            for t in range(1, outer):
                total += land2[c, place.plane(t)].astype(f32)
            span = slice(c * column_chunk, (c + 1) * column_chunk)
            out[:, span] = (residual[:, span] + total).astype(bf16)

    remote(passed, landed, tp_s, tp_r.at[0], tp=sibling).wait_send()
    others = summed.at[:, :, pl.ds(0, inner - 1)]
    remote(others, others, l1_s, l1_r.at[0], ep=me).wait_send()
    others = mid.at[:, pl.ds(0, outer - 1)]
    remote(others, others, l2_s, l2_r.at[0], ep=me).wait_send()


def last_kernel(mixed_in, memory_in, stab_in, mixed, memory, stab, sems):
    pairs = ((memory_in, memory), (mixed_in, mixed), (stab_in, stab))
    moves = [
        pltpu.make_async_copy(source, target, sems.at[i])
        for i, (source, target) in enumerate(pairs)
    ]
    for move in moves:
        move.start()
    for move in moves:
        move.wait()


def in_vmem():
    return pl.BlockSpec(memory_space=pltpu.VMEM)


def in_place():
    return pl.BlockSpec(memory_space=pltpu.HBM)


def held(*arrays):
    return [pltpu.with_memory_space_constraint(array, pltpu.HBM) for array in arrays]


def copies(*numbers):
    return [
        pltpu.SemaphoreType.DMA((number,)) if number else pltpu.SemaphoreType.DMA
        for number in numbers
    ]


def body(
    tokens,
    norm_gain,
    query_weight,
    key_weight,
    value_weight,
    outgate_weight,
    input_weight,
    forget_weight,
    forget_bias,
    memory,
    stabilizer,
    head_gain,
    mix_weight,
    second_gain,
    route_experts,
    route_weight,
    expert_gate,
    expert_up,
    expert_down,
    dense_gate,
    dense_up,
    dense_down,
    branch_scale,
):
    sequences, model_width = tokens.shape
    count = lax.axis_size("ep")
    sides = lax.axis_size("tp")
    inner = 1 << ((count.bit_length() - 1) // 2)
    outer = count // inner
    rows = sequences * count
    half = rows // sides
    width = model_width // count
    heads, size = memory.shape[1], memory.shape[2]
    head_width = query_weight.shape[1]
    part_width = model_width // sides
    topk = route_experts.shape[1]

    aligned = width % lanes == 0
    landing = (sides, half, model_width) if aligned else (count, sides, half, width)
    gates = 2 * heads
    grown = rows // 256

    residual, row_weights, stab_new, memory_new = pl.pallas_call(
        functools.partial(first_kernel, outer, inner),
        out_shape=(
            jax.ShapeDtypeStruct(landing, bf16),
            jax.ShapeDtypeStruct((count, 1, lanes), f32),
            jax.ShapeDtypeStruct((heads, sequences), f32),
            jax.ShapeDtypeStruct(memory.shape, f32),
        ),
        in_specs=[in_place()] * 15,
        out_specs=(in_vmem(),) * 4,
        scratch_shapes=[
            pltpu.VMEM((sequences, model_width), bf16),
            pltpu.VMEM((1, model_width), f32),
            pltpu.VMEM((heads, width, 4 * size), bf16),
            pltpu.VMEM((heads, width), bf16),
            pltpu.VMEM((heads, width), bf16),
            pltpu.VMEM((1, heads), f32),
            pltpu.VMEM((heads, sequences), f32),
            pltpu.VMEM((heads, size), f32),
            pltpu.VMEM((head_width, width), bf16),
            pltpu.VMEM((topk, sequences), jnp.int32),
            pltpu.VMEM((topk, sequences), f32),
            pltpu.VMEM((count, sequences, width), bf16),
            pltpu.VMEM((count, sequences, width), bf16),
            pltpu.VMEM((count, sequences, width), bf16),
            pltpu.VMEM((count // sides, sequences, width), bf16),
            pltpu.VMEM((count, 1, lanes), f32),
            pltpu.VMEM((outer, inner, sequences, lanes), bf16),
            pltpu.VMEM((inner, outer, sequences, lanes), bf16),
            pltpu.VMEM((outer, sequences, lanes), f32),
            pltpu.VMEM((outer, sequences, lanes), f32),
            pltpu.VMEM((heads, outer, inner, sequences, 4 * size), bf16),
            pltpu.VMEM((heads, outer, inner, sequences, 4 * size), bf16),
            pltpu.VMEM((heads, outer, sequences, 2 * size), f32),
            pltpu.VMEM((heads, outer, sequences, 2 * size), f32),
            pltpu.VMEM((heads, outer, sequences, 2 * size), bf16),
            pltpu.VMEM((heads, outer, sequences, 2 * size), bf16),
            pltpu.VMEM((gates, lanes), f32),
            pltpu.VMEM((heads, sequences, lanes), f32),
            pltpu.VMEM((heads, sequences, lanes), f32),
            pltpu.VMEM((heads, count, sequences, size), bf16),
            pltpu.VMEM((sides, half, width), bf16),
            pltpu.VMEM((half, width), bf16),
        ]
        + copies(10, 4 * heads)
        + copies(0, 0, 0, count // sides, 0, 0, 0, 0, 0, 0)
        + copies(0, heads * outer, 0, heads, 0, heads, heads)
        + copies(0, heads, heads, 0, 0, 0, count, 0, 0),
        compiler_params=pltpu.CompilerParams(
            collective_id=1, has_side_effects=True, vmem_limit_bytes=(14 + 8 * grown) * 2**20
        ),
    )(
        *held(
        tokens,
        norm_gain.reshape(1, model_width),
        query_weight,
        key_weight,
        value_weight,
        outgate_weight,
        input_weight.T,
        forget_weight.T,
        forget_bias.reshape(1, heads),
        stabilizer.T,
        head_gain.reshape(heads, size),
        mix_weight,
        route_experts.T,
        route_weight.T,
        memory,
        )
    )
    if not aligned:
        residual = residual.transpose(1, 2, 0, 3)
    residual = residual.reshape(rows, model_width)

    hidden = expert_gate.shape[2]
    dense_rows = dense_gate.shape[0]
    hidden_chunk = min(hidden, 256)
    column_chunk = min(part_width, 256)
    chunks = part_width // column_chunk
    mixed = pl.pallas_call(
        functools.partial(second_kernel, outer, inner, chunks, max(1, rows // 256)),
        out_shape=jax.ShapeDtypeStruct((sequences, part_width), bf16),
        in_specs=[in_vmem()] * 2 + [in_place()] * 8,
        out_specs=in_vmem(),
        scratch_shapes=[
            pltpu.VMEM((1, model_width), f32),
            pltpu.VMEM((1, model_width), f32),
            pltpu.VMEM((hidden // hidden_chunk, model_width, hidden_chunk), bf16),
            pltpu.VMEM((hidden // hidden_chunk, model_width, hidden_chunk), bf16),
            pltpu.VMEM((2 * chunks, hidden, column_chunk), bf16),
            pltpu.VMEM((dense_rows, model_width), bf16),
            pltpu.VMEM((dense_rows, model_width), bf16),
            pltpu.VMEM((dense_rows, model_width), bf16),
            pltpu.VMEM((rows, model_width), bf16),
            pltpu.VMEM((rows, dense_rows), bf16),
            pltpu.VMEM((rows, 1), f32),
            pltpu.VMEM((rows, hidden), bf16),
            pltpu.VMEM((chunks, rows, column_chunk), bf16),
            pltpu.VMEM((chunks, rows, column_chunk), bf16),
            pltpu.VMEM((chunks, rows, column_chunk), f32),
            pltpu.VMEM((chunks, outer, inner, sequences, column_chunk), bf16),
            pltpu.VMEM((chunks, outer, inner, sequences, column_chunk), bf16),
            pltpu.VMEM((chunks, outer, sequences, column_chunk), bf16),
            pltpu.VMEM((chunks, outer, sequences, column_chunk), bf16),
        ]
        + copies(hidden // hidden_chunk, hidden // hidden_chunk, 2 * chunks, 5)
        + copies(0, chunks, 0, chunks * outer, 0, chunks),
        compiler_params=pltpu.CompilerParams(
            collective_id=2, has_side_effects=True, vmem_limit_bytes=(20 + 8 * grown) * 2**20
        ),
    )(
        residual,
        row_weights,
        *held(
            second_gain.reshape(1, model_width),
            branch_scale.reshape(1, model_width),
            expert_gate,
            expert_up,
            expert_down,
            dense_gate,
            dense_up,
            dense_down,
        ),
    )
    mixed, memory_new, stab_new = pl.pallas_call(
        last_kernel,
        out_shape=tuple(
            jax.ShapeDtypeStruct(array.shape, array.dtype)
            for array in (mixed, memory_new, stab_new)
        ),
        in_specs=[in_vmem()] * 3,
        out_specs=(in_place(),) * 3,
        scratch_shapes=copies(3),
        compiler_params=pltpu.CompilerParams(vmem_limit_bytes=8 * 2**20),
    )(mixed, memory_new, stab_new)
    return (mixed, memory_new, stab_new.T)


def solution(mesh):
    in_specs = (
        P("ep", None),
        P(),
        P("ep", "tp"),
        P("ep", "tp"),
        P("ep", "tp"),
        P("ep", "tp"),
        P("ep", "tp"),
        P("ep", "tp"),
        P("tp"),
        P("ep", "tp", None, None),
        P("ep", "tp"),
        P("tp"),
        P("tp", "ep"),
        P(),
        P("ep", None),
        P("ep", None),
        P("ep", None, "tp"),
        P("ep", None, "tp"),
        P("ep", "tp", None),
        P(("ep", "tp"), None),
        P(("ep", "tp"), None),
        P(("ep", "tp"), None),
        P(),
    )
    out_specs = (P("ep", "tp"), P("ep", "tp", None, None), P("ep", "tp"))
    return jax.shard_map(body, mesh=mesh, in_specs=in_specs, out_specs=out_specs, check_vma=False)
```

time: 119 us -> 73.5 us (0.62); the launches traced: 117 us -> 73.3 us
  matrix products: 19.7 us -> 0 us
  other arithmetic: 9.97 us -> 0 us
  Pallas kernels: 80.4 us -> 72.7 us
  waiting for transfers between devices: 4.44 us -> 0 us
  local copies, waits for them, and re-layouts: 1.28 us -> 0 us
    dot_general x8 -> x0, matrix products: 19.7 us -> none  [the longest x1 7.68 us: body(): jnp.dot(expert_act, expert_down[0], preferred_element_type=jnp.float32)]
    pallas_call x5 -> x3, Pallas kernels: 80.4 us -> 72.7 us  [the longest x1 50.5 us: body(): pl.pallas_call(functools.partial(first_kernel, outer, inner), out_shape=(...]
    ppermute x3 -> x0, waiting for transfers between devices: 4.44 us -> none  [the longest x1 1.79 us: body(): other_rows = lax.ppermute(half_rows, 'tp', swap)]
    add x2 -> x0, other arithmetic: 3.12 us -> none  [the longest x1 3.04 us: memory_step(): carried[:, :, None, None] * memory]
    convert_element_type x6 -> x0, other arithmetic: 2.99 us -> none  [the longest x1 1.32 us: body(): summed = (jnp.where(first, left, right) + received).astype(jnp.bfloat16)]
    reduce_sum x5 -> x0, other arithmetic: 2.31 us -> none  [the longest x3 1.36 us: rms_scale(): mean_square = jnp.mean(values * values, axis=-1, keepdims=True)]
  transfers between devices with their start and end apart: 3 -> 0, of which waited for: 3 -> 0; matrix products, arithmetic and copies ran while one was open for 1% -> 0% of each run, Pallas kernels for 0% -> 0%
where the time goes in v1:
time: 73.5 us; the launch traced here: 73.3 us
  Pallas kernels  72.7 us (99%)
    pallas_call x1, Pallas kernels, body(): pl.pallas_call(functools.partial(first_kernel, outer, inner), out_shape=(...  50.5 us
    pallas_call x1, Pallas kernels, body(): pl.pallas_call(functools.partial(second_kernel, outer, inner, chunks, max...  20.1 us
    pallas_call x1, Pallas kernels, body(): pl.pallas_call(last_kernel, out_shape=tuple((jax.ShapeDtypeStruct(array.s...  2.05 us

profile of v1, /device:TPU:0, one launch (start us, length us, event | category | flops | bytes accessed | tf_op | source)
XLA Modules:
  0.0 73.3 jit_solution(13893872441309322695)
XLA Ops:
  0.6 50.5 %shard_map.238 = (bf16[2,128,2048]{2,1,0:T(8,128)(2,1)S(1)}, f32[16,1,128]{2,1,0:T(1,128)S(1)}, f32[4,16]{1,0:T(4,128)S(1)}, f32[16,4,128,128]{3,2,1,0:T(8,128)S(1)}) custom-call(bf16[16,2048]{1,0:T(8,128)(2,1)} %tok_in.1, f32[1,2048]{1,0:T(1,128)} %bitcast.13, bf16[128,512]{1,0:T(8,128)(2,1)} %wq.1, bf16[128,512]{1,0:T(8,128)(2,1)} %wk.1, ...), custom_call_target="tpu_custom_call" | custom-call | tf_op jit(solution)/shard_map/pallas_call | solution.py:894
  51.2 20.1 %shard_map.239.mixed_in = bf16[16,1024]{1,0:T(8,128)(2,1)S(1)} custom-call(bf16[256,2048]{1,0:T(8,128)(2,1)S(1)} %bitcast.12, f32[16,1,128]{2,1,0:T(1,128)S(1)} %get-tuple-element.11.rww, f32[1,2048]{1,0:T(1,128)} %bitcast.14, f32[1,2048]{1,0:T(1,128)} %bitcast.15, bf16[1,2048,1024]{2,1,0:T(8,128)(2,1)} %wg.1, bf16[1,2048,1024]{2,1,0:T(8,128)(2,1)} %wu.1, ...), custom_call_target="tpu_custom_call" | custom-call | tf_op jit(solution)/shard_map/pallas_call | solution.py:973
  71.3 2.0 %shard_map.240 = (bf16[16,1024]{1,0:T(8,128)(2,1)}, f32[16,4,128,128]{3,2,1,0:T(8,128)}, f32[4,16]{1,0:T(4,128)}) custom-call(bf16[16,1024]{1,0:T(8,128)(2,1)S(1)} %shard_map.239.mixed_in, f32[16,4,128,128]{3,2,1,0:T(8,128)S(1)} %get-tuple-element.12.memory_in, f32[4,16]{1,0:T(4,128)S(1)} %get-tuple-element.13.stab_in), custom_call_target="tpu_custom_call" | custom-call | tf_op jit(solution)/shard_map/pallas_call | solution.py:1018

commit v2 on v1

v2 whole, which is shorter than its diff:
```python
import functools

import jax
import jax.numpy as jnp
from jax import lax
from jax.experimental import pallas as pl
from jax.experimental.pallas import tpu as pltpu
from jax.sharding import PartitionSpec as P

norm_eps = 1e-05
clamp_limit = 7.0
sigmoid_slope = 1.702
lanes = 128
f32 = jnp.float32
bf16 = jnp.bfloat16


def loop(lower, upper, step):
    def run(index, carry):
        step(index)
        return carry

    lax.fori_loop(lower, upper, run, 0)


def remote(source, landing, send_sem, recv_sem, **target):
    return pltpu.make_async_remote_copy(
        src_ref=source,
        dst_ref=landing,
        send_sem=send_sem,
        recv_sem=recv_sem,
        device_id=target,
        device_id_type=pl.DeviceIdType.MESH,
    )


def greet(barrier, **target):
    pl.semaphore_signal(
        barrier, inc=1, device_id=target, device_id_type=pl.DeviceIdType.MESH
    )


class Place:
    def __init__(self, outer, inner):
        self.outer, self.inner = outer, inner
        self.me = lax.axis_index("ep")
        self.side = lax.axis_index("tp")
        self.o = self.me // inner
        self.n = self.me % inner

    def plane(self, step):
        return (self.o + step) % self.outer

    def spot(self, step):
        return (self.n + step) % self.inner

    def at(self, plane, spot):
        return plane * self.inner + spot


def gather(place, slot, send_sem, recv_sem, arrived, complete):
    outer, inner, me = place.outer, place.inner, place.me

    def copy(source, target):
        return remote(
            slot(source), slot(source), send_sem, recv_sem.at[source], ep=target
        )

    loop(1, outer, lambda t: copy(me, place.at(place.plane(t), place.n)).start())
    loop(1, inner, lambda u: copy(me, place.at(place.o, place.spot(u))).start())
    arrived(me)

    def relay(t):
        source = place.at(place.plane(t), place.n)
        copy(source, source).wait_recv()
        loop(
            1,
            inner,
            lambda u: copy(source, place.at(place.o, place.spot(u))).start(),
        )
        arrived(source)

    loop(1, outer, relay)

    def take(t):
        def one(u):
            source = place.at(place.plane(t), place.spot(u))
            copy(source, source).wait_recv()
            arrived(source)

        loop(1, inner, one)

    take(0)

    def turn(t):
        take(t)
        complete(t - 1)

    loop(1, outer, turn)
    complete(outer - 1)


def sigmoid(values):
    return 1.0 / (1.0 + jnp.exp(-values))


def first_kernel(
    outer,
    inner,
    tok_in,
    norm_gain_in,
    wq,
    wk,
    wv,
    wo,
    wi_in,
    wf_in,
    bias_in,
    stab_in,
    head_gain_in,
    mix_in,
    rexp_in,
    rwt_in,
    mem_in,
    res,
    rww,
    stab_out,
    mem,
    tok,
    norm_gain,
    wide,
    wi,
    wf,
    bias,
    stab,
    hgain,
    mix,
    rexp,
    rwt,
    nbuf,
    nland,
    tbuf,
    tland,
    rbuf,
    pg,
    gland1,
    gmid,
    gland2,
    pbuf,
    land1,
    mid,
    land2,
    mid_half,
    land2_half,
    turned,
    carried_rows,
    written_rows,
    gland,
    pv,
    came,
    in_s,
    wide_s,
    p1_s,
    p1_r,
    tk_s,
    tk_r,
    rt_s,
    rt_r,
    g1_s,
    g1_r,
    g2_s,
    g2_r,
    l1_s,
    l1_r,
    l2_s,
    l2_r,
    l3_s,
    l3_r,
    mi,
    ag_s,
    ag_r,
    ap_r,
    tp_s,
    tp_r,
    ar_s,
    ar_r,
    sb_s,
    sb_r,
    begin=lambda: None,
    ready=lambda: None,
    group=None,
):
    place = Place(outer, inner)
    me, side, o, n = place.me, place.side, place.o, place.n
    count = outer * inner
    sequences, heads, size = mem.shape[0], mem.shape[1], mem.shape[2]
    width = nland.shape[2]
    rows = count * sequences
    half = pv.shape[1]
    per_half = count // 2
    sibling = 1 - side

    barrier = pltpu.get_barrier_semaphore()
    loop(1, count, lambda t: greet(barrier, ep=(me + t) % count))
    greet(barrier, tp=sibling)
    small = [
        pltpu.make_async_copy(source, target, in_s.at[i])
        for i, (source, target) in enumerate(
            (
                (tok_in, tok),
                (norm_gain_in, norm_gain),
                (rexp_in, rexp),
                (rwt_in, rwt),
                (wi_in, wi),
                (wf_in, wf),
                (bias_in, bias),
                (stab_in, stab),
                (head_gain_in, hgain),
                (mix_in, mix),
            )
        )
    ]
    for copy in small[:6]:
        copy.start()

    def wide_copies(h):
        part = slice(h * size, (h + 1) * size)
        return [
            pltpu.make_async_copy(
                weight.at[:, part],
                wide.at[h, :, slice(j * size, (j + 1) * size)],
                wide_s.at[4 * h + j],
            )
            for j, weight in enumerate((wq, wk, wv, wo))
        ]

    for h in range(heads):
        for copy in wide_copies(h):
            copy.start()
    for copy in small[6:]:
        copy.start()
    loop(
        0,
        heads,
        lambda h: pltpu.make_async_copy(mem_in.at[:, h], mem.at[:, h], mi.at[h]).start(),
    )

    small[0].wait()
    small[1].wait()
    tokens = tok[...].astype(f32)
    mean_square = jnp.mean(tokens * tokens, axis=-1, keepdims=True)
    normed = (tokens * lax.rsqrt(mean_square + norm_eps) * norm_gain[...]).astype(bf16)
    for p in range(count):
        nbuf[p] = normed[:, p * width : (p + 1) * width]

    with jax.named_scope("barrier"):
        pl.semaphore_wait(barrier, count)

    def send_normed(t):
        peer = (me + t) % count
        remote(nbuf.at[peer], nland.at[me], p1_s, p1_r, ep=peer).start()

    loop(1, count, send_normed)
    nland[me] = nbuf[me]

    small[2].wait()
    small[3].wait()
    topk = rexp.shape[0]
    experts = lax.broadcasted_iota(jnp.int32, (count, sequences), 0)
    weights = jnp.zeros((count, sequences), f32)
    for k in range(topk):
        weights += jnp.where(rexp[k : k + 1, :] == experts, rwt[k : k + 1, :], 0.0)
    rbuf[...] = jnp.zeros_like(rbuf)
    for p in range(count):
        rbuf[p, :, :sequences] = weights[p : p + 1, :]

    for p in range(count):
        tbuf[p] = tok[:, p * width : (p + 1) * width]
    begin()
    mine = side == me // per_half

    def token_copy(t):
        peer = (me + t) % count
        return remote(
            tbuf.at[peer], tland.at[me % per_half], tk_s, tk_r.at[me % per_half], ep=peer
        )

    @pl.when(mine)
    def _():
        loop(1, count, lambda t: token_copy(t).start())
        tland[me % per_half] = tbuf[me]

    def send_route(t):
        peer = (me + t) % count
        remote(rbuf.at[peer], rww.at[me], rt_s, rt_r, ep=peer).start()

    loop(1, count, send_route)
    rww[me] = rbuf[me]

    small[4].wait()
    small[5].wait()
    gates = 2 * heads
    once = jnp.concatenate((wi[...].astype(f32), wf[...].astype(f32)), axis=0)
    thin = jnp.concatenate(
        (once, once, jnp.zeros((lanes - 2 * gates, width), f32)), axis=0
    ).astype(bf16)

    with jax.named_scope("normed"):
        others = nland.at[pl.ds(0, count - 1)]
        remote(others, others, p1_s, p1_r, ep=me).wait_recv()
    columns = nland[...].reshape(rows, width)

    lane = lax.broadcasted_iota(jnp.int32, (rows, lanes), 1)
    thin_sums = lax.dot_general(
        columns, thin, (((1,), (1,)), ((), ())), preferred_element_type=f32
    )
    upper = thin_sums.astype(bf16).astype(f32)
    parted = jnp.where(lane < gates, upper, thin_sums - upper).astype(bf16)
    pg[...] = parted.reshape(outer, inner, sequences, lanes)

    def send_gates(t):
        spot = place.spot(t)
        remote(
            pg.at[:, spot], gland1.at[n], g1_s, g1_r, ep=place.at(o, spot)
        ).start()

    loop(1, inner, send_gates)

    def send_part(h, plane):
        def send(t):
            spot = place.spot(t)
            remote(
                pbuf.at[h, plane, spot],
                land1.at[h, plane, n],
                l1_s,
                l1_r.at[h * outer + plane],
                ep=place.at(o, spot),
            ).start()

        loop(1, inner, send)

    for h in range(heads):
        for copy in wide_copies(h):
            copy.wait()
        sums = jnp.dot(columns, wide[h], preferred_element_type=f32).astype(bf16)
        pbuf[h] = sums.reshape(outer, inner, sequences, 4 * size)
        loop(1, outer, lambda t: send_part(h, place.plane(t)))
        if h > 0:
            send_part(h - 1, o)
    send_part(heads - 1, o)
    for copy in small[6:]:
        copy.wait()

    with jax.named_scope("gates"):
        others = gland1.at[pl.ds(0, inner - 1)]
        remote(others, others, g1_s, g1_r, ep=me).wait_recv()
    for a in range(outer):
        total = pg[a, n].astype(f32)
        for t in range(1, inner):
            total += gland1[place.spot(t), a].astype(f32)
        gmid[a] = total

    def pass_gates(t):
        plane = place.plane(t)
        remote(
            gmid.at[plane], gland2.at[o], g2_s, g2_r, ep=place.at(plane, n)
        ).start()

    loop(1, outer, pass_gates)

    def plane_sum(h, plane):
        with jax.named_scope("first"):
            others = land1.at[h, plane, pl.ds(0, inner - 1)]
            remote(others, others, l1_s, l1_r.at[h * outer + plane], ep=me).wait_recv()
        total = pbuf[h, plane, n].astype(f32)
        for t in range(1, inner):
            total += land1[h, plane, place.spot(t)].astype(f32)
        return total

    def first_sum(h):
        def send(t):
            plane = place.plane(t)
            total = plane_sum(h, plane)
            mid[h, plane] = total[:, : 2 * size]
            mid_half[h, plane] = total[:, 2 * size :].astype(bf16)
            target = place.at(plane, n)
            remote(mid.at[h, plane], land2.at[h, o], l2_s, l2_r.at[h], ep=target).start()
            remote(
                mid_half.at[h, plane], land2_half.at[h, o], l3_s, l3_r.at[h], ep=target
            ).start()

        loop(1, outer, send)

    def gate_math():
        with jax.named_scope("gates2"):
            others = gland2.at[pl.ds(0, outer - 1)]
            remote(others, others, g2_s, g2_r, ep=me).wait_recv()
        total = gmid[o]
        for t in range(1, outer):
            total += gland2[place.plane(t)]
        turn = jnp.transpose(total)
        turn = turn[:gates] + turn[gates : 2 * gates]
        input_pre, forget_pre = turn[:heads], turn[heads:]
        square = lax.broadcasted_iota(jnp.int32, (heads, heads), 0) == lax.broadcasted_iota(
            jnp.int32, (heads, heads), 1
        )
        shift = jnp.sum(jnp.where(square, bias[...], 0.0), axis=1, keepdims=True)
        shifted = forget_pre + shift
        log_forget = jnp.minimum(shifted, 0.0) - jnp.log1p(jnp.exp(-jnp.abs(shifted)))
        stab_new = jnp.maximum(log_forget + stab[...], input_pre)
        stab_out[...] = stab_new
        turned[...] = jnp.zeros_like(turned)
        turned[:heads, :sequences] = jnp.exp(log_forget + stab[...] - stab_new)
        turned[heads:gates, :sequences] = jnp.exp(input_pre - stab_new) * size**-0.5
        back = jnp.transpose(turned[...])[:sequences]
        for h in range(heads):
            carried_rows[h] = jnp.broadcast_to(back[:, h : h + 1], (sequences, lanes))
            written_rows[h] = jnp.broadcast_to(
                back[:, heads + h : heads + h + 1], (sequences, lanes)
            )

    def memory_head(h):
        own = plane_sum(h, o)
        with jax.named_scope("heads"):
            others = land2.at[h, pl.ds(0, outer - 1)]
            remote(others, others, l2_s, l2_r.at[h], ep=me).wait_recv()
            others = land2_half.at[h, pl.ds(0, outer - 1)]
            remote(others, others, l3_s, l3_r.at[h], ep=me).wait_recv()
        pltpu.make_async_copy(mem_in.at[:, h], mem.at[:, h], mi.at[h]).wait()
        query_key, value_gate = own[:, : 2 * size], own[:, 2 * size :]
        for t in range(1, outer):
            query_key += land2[h, place.plane(t)]
            value_gate += land2_half[h, place.plane(t)].astype(f32)
        query_key = query_key.astype(bf16)
        value_gate = value_gate.astype(bf16).astype(f32)
        query, key = query_key[:, :size], query_key[:, size:]
        value, outgate = value_gate[:, :size], value_gate[:, size:]
        value_columns = jnp.transpose(value)
        places = lax.broadcasted_iota(jnp.int32, (size, sequences), 1)
        lines = lax.broadcasted_iota(jnp.int32, (sequences, size), 0)
        across = (((1,), (1,)), ((), ()))

        def some(group, readout):
            for i in range(unroll):
                s = group * unroll + i
                column = jnp.where(places == s, value_columns, 0.0).astype(bf16)
                product = jnp.dot(column, key, preferred_element_type=f32)
                carry = carried_rows[h, pl.ds(s, 1), :]
                write = written_rows[h, pl.ds(s, 1), :]
                updated = carry * mem[s, h] + write * product
                mem[s, h] = updated
                upper = updated.astype(bf16)
                under = (updated - upper.astype(f32)).astype(bf16)
                answers = lax.dot_general(query, upper, across, preferred_element_type=f32)
                answers += lax.dot_general(query, under, across, preferred_element_type=f32)
                readout = jnp.where(lines == s, answers, readout)
            return readout

        unroll = min(sequences, 8)
        readout = lax.fori_loop(
            0, sequences // unroll, some, jnp.zeros((sequences, size), f32)
        )
        mean_square = jnp.mean(readout * readout, axis=-1, keepdims=True)
        gated = (
            readout
            * lax.rsqrt(mean_square + norm_eps)
            * hgain[pl.ds(h, 1), :]
            * sigmoid(outgate)
        )
        gland[h, me] = gated.astype(bf16)
        block = gland.at[h, me]
        loop(
            1,
            outer,
            lambda t: remote(
                block, block, ag_s, ag_r.at[h], ep=place.at(place.plane(t), n)
            ).start(),
        )
        loop(
            1,
            inner,
            lambda u: remote(
                block, block, ag_s, ap_r.at[h], ep=place.at(o, place.spot(u))
            ).start(),
        )

    def relay(h):
        others = gland.at[h, pl.ds(0, outer - 1)]
        remote(others, others, ag_s, ag_r.at[h], ep=me).wait_recv()

        def one(t):
            block = gland.at[h, place.at(place.plane(t), n)]
            loop(
                1,
                inner,
                lambda u: remote(
                    block, block, ag_s, ap_r.at[h], ep=place.at(o, place.spot(u))
                ).start(),
            )

        loop(1, outer, one)

    def head_step(h):
        @pl.when(h < heads)
        def _():
            first_sum(h)

        @pl.when(h == 0)
        def _():
            gate_math()

        @pl.when(h > 0)
        def _():
            memory_head(h - 1)

    loop(0, heads + 1, head_step)

    with jax.named_scope("gated"):
        loop(0, heads, relay)
        partial = jnp.zeros((rows, width), f32)
        for h in range(heads):
            others = gland.at[h, pl.ds(0, outer * (inner - 1))]
            remote(others, others, ag_s, ap_r.at[h], ep=me).wait_recv()
            partial += jnp.dot(
                gland[h].reshape(rows, size),
                mix[h * size : (h + 1) * size, :],
                preferred_element_type=f32,
            )
        partial = partial.astype(bf16)
    pv[...] = partial.reshape(2, half, width)
    swap = remote(pv.at[sibling], came, tp_s, tp_r, tp=sibling)
    swap.start()

    def take_tokens(b):
        source = side * per_half + b

        @pl.when(source != me)
        def _():
            remote(tland.at[b], tland.at[b], tk_s, tk_r.at[b], ep=source).wait_recv()

    loop(0, per_half, take_tokens)
    with jax.named_scope("swap"):
        swap.wait_recv()
    attended = pv[side].astype(f32) + came[...].astype(f32)
    residual = (tland[...].reshape(half, width).astype(f32) + attended).astype(bf16)
    def slot(p, core):
        if len(res.shape) == 2:
            return res.at[
                pl.ds(pl.multiple_of(core * half, half), half),
                pl.ds(pl.multiple_of(p * width, width), width),
            ]
        return res.at[p, core]

    slot(me, side)[...] = residual

    def hand(p):
        remote(slot(p, side), slot(p, side), sb_s, sb_r.at[p // inner], tp=sibling).start()

    def complete(t):
        plane = place.plane(t)
        if len(res.shape) == 2:
            across = pl.ds(pl.multiple_of(plane * inner * width, inner * width), inner * width)
            whole = res.at[pl.ds(pl.multiple_of(sibling * half, half), half), across]
        else:
            whole = res.at[pl.ds(plane * inner, inner), sibling]
        with jax.named_scope("settle"):
            remote(whole, whole, sb_s, sb_r.at[plane], tp=sibling).wait_recv()
        if group is not None:
            group(plane)

    ready()
    others = rww.at[pl.ds(0, count - 1)]
    remote(others, others, rt_s, rt_r, ep=me).wait()
    with jax.named_scope("rows"):
        gather(place, lambda p: slot(p, side), ar_s, ar_r, hand, complete)

    def settle():
        if len(res.shape) == 2:
            rows_side = pl.ds(pl.multiple_of(side * half, half), half)
            whole, sent = res.at[rows_side], res.at[rows_side, pl.ds(0, (count - 1) * width)]
        else:
            whole, sent = res.at[:, side], res.at[pl.ds(0, count - 1), side]
        remote(whole, whole, sb_s, sb_r.at[0], tp=sibling).wait_send()
        remote(sent, sent, ar_s, ar_r.at[0], ep=me).wait_send()
        others = nbuf.at[pl.ds(0, count - 1)]
        remote(others, others, p1_s, p1_r, ep=me).wait_send()

        @pl.when(mine)
        def _():
            remote(others, others, tk_s, tk_r.at[0], ep=me).wait_send()

        others = gland1.at[pl.ds(0, inner - 1)]
        remote(others, others, g1_s, g1_r, ep=me).wait_send()
        others = gmid.at[pl.ds(0, outer - 1)]
        remote(others, others, g2_s, g2_r, ep=me).wait_send()
        others = pbuf.at[:, :, pl.ds(0, inner - 1)]
        remote(others, others, l1_s, l1_r.at[0], ep=me).wait_send()
        others = mid.at[:, pl.ds(0, outer - 1)]
        remote(others, others, l2_s, l2_r.at[0], ep=me).wait_send()
        others = mid_half.at[:, pl.ds(0, outer - 1)]
        remote(others, others, l3_s, l3_r.at[0], ep=me).wait_send()
        others = gland.at[:, pl.ds(0, count - 1)]
        remote(others, others, ag_s, ag_r.at[0], ep=me).wait_send()
        swap.wait_send()

    return settle


def second_kernel(
    outer,
    inner,
    chunks,
    row_blocks,
    res,
    rww,
    gain_in,
    scale_in,
    wg,
    wu,
    wd,
    dg,
    du,
    dd,
    out,
    gain,
    scale,
    wgv,
    wuv,
    wdv,
    dgv,
    duv,
    ddv,
    gate_sum,
    up_sum,
    dense_gate_sum,
    dense_up_sum,
    squares,
    dense_act,
    row_weight,
    act,
    passed,
    landed,
    kept,
    summed,
    land1,
    mid,
    land2,
    wg_m,
    wu_m,
    wd_m,
    d_m,
    tp_s,
    tp_r,
    l1_s,
    l1_r,
    l2_s,
    l2_r,
):
    place = Place(outer, inner)
    me, side, o, n = place.me, place.side, place.o, place.n
    count = outer * inner
    rows, model_width = res.shape
    sequences = rows // count
    sibling = 1 - side
    hidden_chunk = wgv.shape[2]
    column_chunk = wdv.shape[2]
    part_width = chunks * column_chunk

    dense = [
        pltpu.make_async_copy(source, target, d_m.at[i])
        for i, (source, target) in enumerate(
            ((dg, dgv), (du, duv), (dd, ddv), (gain_in, gain), (scale_in, scale))
        )
    ]
    hidden_chunks = wgv.shape[0]

    def gate_copy(c):
        span = pl.ds(c * hidden_chunk, hidden_chunk)
        return pltpu.make_async_copy(wg.at[0, :, span], wgv.at[c], wg_m.at[c])

    def up_copy(c):
        span = pl.ds(c * hidden_chunk, hidden_chunk)
        return pltpu.make_async_copy(wu.at[0, :, span], wuv.at[c], wu_m.at[c])

    def down_copy(c):
        span = pl.ds(c * column_chunk, column_chunk)
        return pltpu.make_async_copy(wd.at[0, :, span], wdv.at[c], wd_m.at[c])

    block = act.shape[0] // row_blocks
    across = model_width // outer

    def part(r):
        return pl.ds(pl.multiple_of(r * block, block), block)

    def begin():
        dense[3].start()
        for c in range(hidden_chunks):
            gate_copy(c).start()
            up_copy(c).start()
        for c in (0, 1, 2, 4):
            dense[c].start()
        for c in range(chunks):
            down_copy(sibling * chunks + c).start()
            down_copy(side * chunks + c).start()
        for sums in (gate_sum, up_sum, dense_gate_sum, dense_up_sum, squares):
            sums[...] = jnp.zeros_like(sums)

    def arrive():
        dense[3].wait()
        dense[0].wait()
        dense[1].wait()
        for c in range(hidden_chunks):
            gate_copy(c).wait()
            up_copy(c).wait()

    turned = (((1,), (1,)), ((), ()))

    def group(plane):
        span = pl.ds(pl.multiple_of(plane * across, across), across)

        def one(r):
            values = res[part(r), span].astype(f32)
            squares[part(r), :] += jnp.sum(values * values, axis=-1, keepdims=True)
            scaled = (values * gain[:, span]).astype(bf16)
            for c in range(hidden_chunks):
                gate_sum[c, part(r), :] += jnp.dot(
                    scaled, wgv[c, span, :], preferred_element_type=f32
                )
                up_sum[c, part(r), :] += jnp.dot(
                    scaled, wuv[c, span, :], preferred_element_type=f32
                )
            dense_gate_sum[part(r), :] += lax.dot_general(
                scaled, dgv[:, span], turned, preferred_element_type=f32
            )
            dense_up_sum[part(r), :] += lax.dot_general(
                scaled, duv[:, span], turned, preferred_element_type=f32
            )

        with jax.named_scope("group"):
            loop(0, row_blocks, one)

    def products():
        received = jnp.broadcast_to(rww[...], (count, sequences, lanes)).reshape(rows, lanes)
        line = lax.broadcasted_iota(jnp.int32, (rows, lanes), 0) % sequences
        lane = lax.broadcasted_iota(jnp.int32, (rows, lanes), 1)
        row_weight[...] = jnp.sum(jnp.where(line == lane, received, 0.0), axis=-1, keepdims=True)

        row_scale = lax.rsqrt(squares[...] / model_width + norm_eps)
        squares[...] = row_scale

        def activate(r):
            scale_rows = squares[part(r), :]
            gate_rows = dense_gate_sum[part(r), :] * scale_rows
            lift_rows = dense_up_sum[part(r), :] * scale_rows
            dense_act[part(r), :] = (gate_rows * sigmoid(gate_rows) * lift_rows).astype(bf16)
            for c in range(hidden_chunks):
                gate_pre = jnp.minimum(gate_sum[c, part(r), :] * scale_rows, clamp_limit)
                up_pre = jnp.clip(up_sum[c, part(r), :] * scale_rows, -clamp_limit, clamp_limit)
                act[part(r), c * hidden_chunk : (c + 1) * hidden_chunk] = (
                    (up_pre + 1.0) * gate_pre * sigmoid(sigmoid_slope * gate_pre)
                ).astype(bf16)

        with jax.named_scope("hidden"):
            loop(0, row_blocks, activate)

        dense[2].wait()
        dense[4].wait()

        def term(c, r):
            span = pl.ds(pl.multiple_of(c * column_chunk, column_chunk), column_chunk)
            routed = jnp.dot(act[part(r), :], wdv[c], preferred_element_type=f32)
            dense_out = jnp.dot(dense_act[part(r), :], ddv[:, span], preferred_element_type=f32)
            return dense_out * scale[:, span] + row_weight[part(r), :] * routed

        def cross(c):
            return remote(passed.at[c], landed.at[c], tp_s, tp_r.at[c], tp=sibling)

        def spread_plane(c, plane):
            def send(t):
                spot = place.spot(t)
                remote(
                    summed.at[c, plane, spot],
                    land1.at[c, plane, n],
                    l1_s,
                    l1_r.at[c * outer + plane],
                    ep=place.at(o, spot),
                ).start()

            loop(1, inner, send)

        def spread(c):
            cross(c).wait_recv()
            both = kept[c] + landed[c].astype(f32)
            summed[c] = both.astype(bf16).reshape(outer, inner, sequences, column_chunk)

            loop(1, outer, lambda t: spread_plane(c, place.plane(t)))

        def give_step(c):
            down_copy(sibling * chunks + c).wait()

            def give(r):
                passed[c, part(r), :] = term(sibling * chunks + c, r).astype(bf16)

            loop(0, row_blocks, give)
            cross(c).start()

        def keep_step(c):
            down_copy(side * chunks + c).wait()

            def keep(r):
                kept[c, part(r), :] = term(side * chunks + c, r)

            loop(0, row_blocks, keep)
            spread(c)

        with jax.named_scope("give"):
            give_step(0)

            def turn(c):
                give_step(c)
                keep_step(c - 1)

            loop(1, chunks, turn)
        with jax.named_scope("keep"):
            keep_step(chunks - 1)

        loop(0, chunks, lambda c: spread_plane(c, o))

        def plane_sum(c, plane):
            others = land1.at[c, plane, pl.ds(0, inner - 1)]
            remote(others, others, l1_s, l1_r.at[c * outer + plane], ep=me).wait_recv()
            total = summed[c, plane, n].astype(f32)
            for t in range(1, inner):
                total += land1[c, plane, place.spot(t)].astype(f32)
            return total

        def first_sum(c):
            def send(t):
                plane = place.plane(t)
                mid[c, plane] = plane_sum(c, plane).astype(bf16)
                remote(
                    mid.at[c, plane], land2.at[c, o], l2_s, l2_r.at[c], ep=place.at(plane, n)
                ).start()

            loop(1, outer, send)

        with jax.named_scope("sum1"):
            loop(0, chunks, first_sum)

        residual = res[
            pl.ds(pl.multiple_of(me * sequences, sequences), sequences),
            pl.ds(pl.multiple_of(side * part_width, part_width), part_width),
        ].astype(f32)

        with jax.named_scope("sum2"):
            for c in range(chunks):
                total = plane_sum(c, o)
                others = land2.at[c, pl.ds(0, outer - 1)]
                remote(others, others, l2_s, l2_r.at[c], ep=me).wait_recv()
                for t in range(1, outer):
                    total += land2[c, place.plane(t)].astype(f32)
                span = slice(c * column_chunk, (c + 1) * column_chunk)
                out[:, span] = (residual[:, span] + total).astype(bf16)

    def settle():
        remote(passed, landed, tp_s, tp_r.at[0], tp=sibling).wait_send()
        others = summed.at[:, :, pl.ds(0, inner - 1)]
        remote(others, others, l1_s, l1_r.at[0], ep=me).wait_send()
        others = mid.at[:, pl.ds(0, outer - 1)]
        remote(others, others, l2_s, l2_r.at[0], ep=me).wait_send()

    def finish():
        products()
        return settle

    return begin, arrive, group, finish


def alone_kernel(outer, inner, *refs):
    first_kernel(outer, inner, *refs)()


def experts_kernel(outer, inner, chunks, row_blocks, *refs):
    place = Place(outer, inner)
    barrier = pltpu.get_barrier_semaphore()
    loop(1, inner, lambda u: greet(barrier, ep=place.at(place.o, place.spot(u))))
    loop(1, outer, lambda t: greet(barrier, ep=place.at(place.plane(t), place.n)))
    greet(barrier, tp=1 - place.side)
    begin, arrive, group, finish = second_kernel(outer, inner, chunks, row_blocks, *refs)
    begin()
    arrive()
    loop(0, outer, group)
    pl.semaphore_wait(barrier, inner + outer - 1)
    finish()()


def whole_kernel(outer, inner, chunks, row_blocks, firsts, *refs):
    first_in, second_in, refs = refs[:15], refs[15:23], refs[23:]
    (mixed, stab_out, mem), (res, rww), refs = refs[:3], refs[3:5], refs[5:]
    begin, arrive, group, finish = second_kernel(
        outer, inner, chunks, row_blocks, res, rww, *second_in, mixed, *refs[firsts:]
    )
    settle = first_kernel(
        outer,
        inner,
        *first_in,
        res,
        rww,
        stab_out,
        mem,
        *refs[:firsts],
        begin=begin,
        ready=arrive,
        group=group,
    )
    finish()()
    settle()


def last_kernel(mixed_in, memory_in, stab_in, mixed, memory, stab, sems):
    pairs = ((memory_in, memory), (mixed_in, mixed), (stab_in, stab))
    moves = [
        pltpu.make_async_copy(source, target, sems.at[i])
        for i, (source, target) in enumerate(pairs)
    ]
    for move in moves:
        move.start()
    for move in moves:
        move.wait()


def in_vmem():
    return pl.BlockSpec(memory_space=pltpu.VMEM)


def in_place():
    return pl.BlockSpec(memory_space=pltpu.HBM)


def held(*arrays):
    return [pltpu.with_memory_space_constraint(array, pltpu.HBM) for array in arrays]


def copies(*numbers):
    return [
        pltpu.SemaphoreType.DMA((number,)) if number else pltpu.SemaphoreType.DMA
        for number in numbers
    ]


def body(
    tokens,
    norm_gain,
    query_weight,
    key_weight,
    value_weight,
    outgate_weight,
    input_weight,
    forget_weight,
    forget_bias,
    memory,
    stabilizer,
    head_gain,
    mix_weight,
    second_gain,
    route_experts,
    route_weight,
    expert_gate,
    expert_up,
    expert_down,
    dense_gate,
    dense_up,
    dense_down,
    branch_scale,
):
    sequences, model_width = tokens.shape
    count = lax.axis_size("ep")
    sides = lax.axis_size("tp")
    inner = 1 << ((count.bit_length() - 1) // 2)
    outer = count // inner
    rows = sequences * count
    half = rows // sides
    width = model_width // count
    heads, size = memory.shape[1], memory.shape[2]
    head_width = query_weight.shape[1]
    part_width = model_width // sides
    topk = route_experts.shape[1]

    aligned = width % lanes == 0
    landing = (sides, half, model_width) if aligned else (count, sides, half, width)
    gates = 2 * heads
    grown = rows // 256

    hidden = expert_gate.shape[2]
    dense_rows = dense_gate.shape[0]
    hidden_chunk = min(hidden, 256)
    column_chunk = min(part_width, 256)
    chunks = part_width // column_chunk
    row_blocks = max(1, grown)
    first_scratch = [
        pltpu.VMEM((sequences, model_width), bf16),
        pltpu.VMEM((1, model_width), f32),
        pltpu.VMEM((heads, width, 4 * size), bf16),
        pltpu.VMEM((heads, width), bf16),
        pltpu.VMEM((heads, width), bf16),
        pltpu.VMEM((1, heads), f32),
        pltpu.VMEM((heads, sequences), f32),
        pltpu.VMEM((heads, size), f32),
        pltpu.VMEM((head_width, width), bf16),
        pltpu.VMEM((topk, sequences), jnp.int32),
        pltpu.VMEM((topk, sequences), f32),
        pltpu.VMEM((count, sequences, width), bf16),
        pltpu.VMEM((count, sequences, width), bf16),
        pltpu.VMEM((count, sequences, width), bf16),
        pltpu.VMEM((count // sides, sequences, width), bf16),
        pltpu.VMEM((count, 1, lanes), f32),
        pltpu.VMEM((outer, inner, sequences, lanes), bf16),
        pltpu.VMEM((inner, outer, sequences, lanes), bf16),
        pltpu.VMEM((outer, sequences, lanes), f32),
        pltpu.VMEM((outer, sequences, lanes), f32),
        pltpu.VMEM((heads, outer, inner, sequences, 4 * size), bf16),
        pltpu.VMEM((heads, outer, inner, sequences, 4 * size), bf16),
        pltpu.VMEM((heads, outer, sequences, 2 * size), f32),
        pltpu.VMEM((heads, outer, sequences, 2 * size), f32),
        pltpu.VMEM((heads, outer, sequences, 2 * size), bf16),
        pltpu.VMEM((heads, outer, sequences, 2 * size), bf16),
        pltpu.VMEM((gates, lanes), f32),
        pltpu.VMEM((heads, sequences, lanes), f32),
        pltpu.VMEM((heads, sequences, lanes), f32),
        pltpu.VMEM((heads, count, sequences, size), bf16),
        pltpu.VMEM((sides, half, width), bf16),
        pltpu.VMEM((half, width), bf16),
    ]
    first_scratch += copies(10, 4 * heads)
    first_scratch += copies(0, 0, 0, count // sides, 0, 0, 0, 0, 0, 0)
    first_scratch += copies(0, heads * outer, 0, heads, 0, heads, heads)
    first_scratch += copies(0, heads, heads, 0, 0, 0, count, 0, outer)
    second_scratch = [
        pltpu.VMEM((1, model_width), f32),
        pltpu.VMEM((1, model_width), f32),
        pltpu.VMEM((hidden // hidden_chunk, model_width, hidden_chunk), bf16),
        pltpu.VMEM((hidden // hidden_chunk, model_width, hidden_chunk), bf16),
        pltpu.VMEM((2 * chunks, hidden, column_chunk), bf16),
        pltpu.VMEM((dense_rows, model_width), bf16),
        pltpu.VMEM((dense_rows, model_width), bf16),
        pltpu.VMEM((dense_rows, model_width), bf16),
        pltpu.VMEM((hidden // hidden_chunk, rows, hidden_chunk), f32),
        pltpu.VMEM((hidden // hidden_chunk, rows, hidden_chunk), f32),
        pltpu.VMEM((rows, dense_rows), f32),
        pltpu.VMEM((rows, dense_rows), f32),
        pltpu.VMEM((rows, 1), f32),
        pltpu.VMEM((rows, dense_rows), bf16),
        pltpu.VMEM((rows, 1), f32),
        pltpu.VMEM((rows, hidden), bf16),
        pltpu.VMEM((chunks, rows, column_chunk), bf16),
        pltpu.VMEM((chunks, rows, column_chunk), bf16),
        pltpu.VMEM((chunks, rows, column_chunk), f32),
        pltpu.VMEM((chunks, outer, inner, sequences, column_chunk), bf16),
        pltpu.VMEM((chunks, outer, inner, sequences, column_chunk), bf16),
        pltpu.VMEM((chunks, outer, sequences, column_chunk), bf16),
        pltpu.VMEM((chunks, outer, sequences, column_chunk), bf16),
    ]
    second_scratch += copies(hidden // hidden_chunk, hidden // hidden_chunk, 2 * chunks, 5)
    second_scratch += copies(0, chunks, 0, chunks * outer, 0, chunks)
    first_arguments = held(
        tokens,
        norm_gain.reshape(1, model_width),
        query_weight,
        key_weight,
        value_weight,
        outgate_weight,
        input_weight.T,
        forget_weight.T,
        forget_bias.reshape(1, heads),
        stabilizer.T,
        head_gain.reshape(heads, size),
        mix_weight,
        route_experts.T,
        route_weight.T,
        memory,
    )
    second_arguments = held(
        second_gain.reshape(1, model_width),
        branch_scale.reshape(1, model_width),
        expert_gate,
        expert_up,
        expert_down,
        dense_gate,
        dense_up,
        dense_down,
    )
    mixed_shape = jax.ShapeDtypeStruct((sequences, part_width), bf16)
    stab_shape = jax.ShapeDtypeStruct((heads, sequences), f32)
    memory_shape = jax.ShapeDtypeStruct(memory.shape, f32)
    if aligned:
        mixed, stab_new, memory_new = pl.pallas_call(
            functools.partial(
                whole_kernel, outer, inner, chunks, row_blocks, len(first_scratch)
            ),
            out_shape=(mixed_shape, stab_shape, memory_shape),
            in_specs=[in_place()] * 23,
            out_specs=(in_vmem(),) * 3,
            scratch_shapes=[
                pltpu.VMEM((rows, model_width), bf16),
                pltpu.VMEM((count, 1, lanes), f32),
            ]
            + first_scratch
            + second_scratch,
            compiler_params=pltpu.CompilerParams(
                collective_id=1, has_side_effects=True, vmem_limit_bytes=44 * 2**20
            ),
        )(*first_arguments, *second_arguments)
    else:
        residual, row_weights, stab_new, memory_new = pl.pallas_call(
            functools.partial(alone_kernel, outer, inner),
            out_shape=(
                jax.ShapeDtypeStruct((count, sides, half, width), bf16),
                jax.ShapeDtypeStruct((count, 1, lanes), f32),
                stab_shape,
                memory_shape,
            ),
            in_specs=[in_place()] * 15,
            out_specs=(in_vmem(),) * 4,
            scratch_shapes=first_scratch,
            compiler_params=pltpu.CompilerParams(
                collective_id=1, has_side_effects=True, vmem_limit_bytes=46 * 2**20
            ),
        )(*first_arguments)
        residual = residual.transpose(1, 2, 0, 3).reshape(rows, model_width)
        mixed = pl.pallas_call(
            functools.partial(experts_kernel, outer, inner, chunks, row_blocks),
            out_shape=mixed_shape,
            in_specs=[in_vmem()] * 2 + [in_place()] * 8,
            out_specs=in_vmem(),
            scratch_shapes=second_scratch,
            compiler_params=pltpu.CompilerParams(
                collective_id=2, has_side_effects=True, vmem_limit_bytes=56 * 2**20
            ),
        )(residual, row_weights, *second_arguments)

    mixed, memory_new, stab_new = pl.pallas_call(
        last_kernel,
        out_shape=tuple(
            jax.ShapeDtypeStruct(array.shape, array.dtype)
            for array in (mixed, memory_new, stab_new)
        ),
        in_specs=[in_vmem()] * 3,
        out_specs=(in_place(),) * 3,
        scratch_shapes=copies(3),
        compiler_params=pltpu.CompilerParams(vmem_limit_bytes=8 * 2**20),
    )(mixed, memory_new, stab_new)
    return (mixed, memory_new, stab_new.T)


def solution(mesh):
    in_specs = (
        P("ep", None),
        P(),
        P("ep", "tp"),
        P("ep", "tp"),
        P("ep", "tp"),
        P("ep", "tp"),
        P("ep", "tp"),
        P("ep", "tp"),
        P("tp"),
        P("ep", "tp", None, None),
        P("ep", "tp"),
        P("tp"),
        P("tp", "ep"),
        P(),
        P("ep", None),
        P("ep", None),
        P("ep", None, "tp"),
        P("ep", None, "tp"),
        P("ep", "tp", None),
        P(("ep", "tp"), None),
        P(("ep", "tp"), None),
        P(("ep", "tp"), None),
        P(),
    )
    out_specs = (P("ep", "tp"), P("ep", "tp", None, None), P("ep", "tp"))
    return jax.shard_map(body, mesh=mesh, in_specs=in_specs, out_specs=out_specs, check_vma=False)
```

time: 73.5 us -> 67.7 us (0.921)
  Pallas kernels: 72.7 us -> 66.9 us
    pallas_call x2 -> x1, Pallas kernels: 70.6 us -> 64.9 us  [body(): pl.pallas_call(functools.partial(whole_kernel, outer, inner, chunks, row_...]
where the time goes in v2:
time: 67.7 us; the launch traced here: 67.6 us
  Pallas kernels  66.9 us (99%)
    pallas_call x1, Pallas kernels, body(): pl.pallas_call(functools.partial(whole_kernel, outer, inner, chunks, row_...  64.9 us
    pallas_call x1, Pallas kernels, body(): pl.pallas_call(last_kernel, out_shape=tuple((jax.ShapeDtypeStruct(array.s...  2.05 us

profile of v2, /device:TPU:0, one launch (start us, length us, event | category | flops | bytes accessed | tf_op | source)
XLA Modules:
  0.0 67.6 jit_solution(14446623050884581244)
XLA Ops:
  0.6 64.9 %shard_map.238 = (bf16[16,1024]{1,0:T(8,128)(2,1)S(1)}, f32[4,16]{1,0:T(4,128)S(1)}, f32[16,4,128,128]{3,2,1,0:T(8,128)S(1)}) custom-call(bf16[16,2048]{1,0:T(8,128)(2,1)} %refs_0_.1, f32[1,2048]{1,0:T(1,128)} %bitcast.11, bf16[128,512]{1,0:T(8,128)(2,1)} %refs_2_.1, bf16[128,512]{1,0:T(8,128)(2,1)} %refs_3_.1, bf16[128,512]{1,0:T(8,128)(2,1)} %refs_4_.1, ...), custom_call_target="tpu_custom_call" | custom-call | tf_op jit(solution)/shard_map/pallas_call | solution.py:1096
  65.5 2.0 %shard_map.239 = (bf16[16,1024]{1,0:T(8,128)(2,1)}, f32[16,4,128,128]{3,2,1,0:T(8,128)}, f32[4,16]{1,0:T(4,128)}) custom-call(bf16[16,1024]{1,0:T(8,128)(2,1)S(1)} %get-tuple-element.9.mixed_in, f32[16,4,128,128]{3,2,1,0:T(8,128)S(1)} %get-tuple-element.10.memory_in, f32[4,16]{1,0:T(4,128)S(1)} %get-tuple-element.11.stab_in), custom_call_target="tpu_custom_call" | custom-call | tf_op jit(solution)/shard_map/pallas_call | solution.py:1141

commit v3 on v2

--- a/solution.py
+++ b/solution.py
@@ -58,25 +58,25 @@
         return plane * self.inner + spot
 
 
-def gather(place, slot, send_sem, recv_sem, arrived, complete):
+def gather(place, slot, plane_sem, spot_sem, recv_sem, arrived, complete):
     outer, inner, me = place.outer, place.inner, place.me
 
-    def copy(source, target):
+    def copy(source, target, send_sem):
         return remote(
             slot(source), slot(source), send_sem, recv_sem.at[source], ep=target
         )
 
-    loop(1, outer, lambda t: copy(me, place.at(place.plane(t), place.n)).start())
-    loop(1, inner, lambda u: copy(me, place.at(place.o, place.spot(u))).start())
+    loop(1, outer, lambda t: copy(me, place.at(place.plane(t), place.n), plane_sem).start())
+    loop(1, inner, lambda u: copy(me, place.at(place.o, place.spot(u)), spot_sem).start())
     arrived(me)
 
     def relay(t):
         source = place.at(place.plane(t), place.n)
-        copy(source, source).wait_recv()
+        copy(source, source, spot_sem).wait_recv()
         loop(
             1,
             inner,
-            lambda u: copy(source, place.at(place.o, place.spot(u))).start(),
+            lambda u: copy(source, place.at(place.o, place.spot(u)), spot_sem).start(),
         )
         arrived(source)
 
@@ -85,7 +85,7 @@
     def take(t):
         def one(u):
             source = place.at(place.plane(t), place.spot(u))
-            copy(source, source).wait_recv()
+            copy(source, source, spot_sem).wait_recv()
             arrived(source)
 
         loop(1, inner, one)
@@ -158,6 +158,7 @@
     gland,
     pv,
     came,
+    mixp,
     in_s,
     wide_s,
     p1_s,
@@ -186,6 +187,10 @@
     ar_r,
     sb_s,
     sb_r,
+    mx_s,
+    mx_r,
+    ar_p,
+    planar=False,
     begin=lambda: None,
     ready=lambda: None,
     group=None,
@@ -196,7 +201,8 @@
     sequences, heads, size = mem.shape[0], mem.shape[1], mem.shape[2]
     width = nland.shape[2]
     rows = count * sequences
-    half = pv.shape[1]
+    half = rows // 2
+    part_spots = inner // 2
     per_half = count // 2
     sibling = 1 - side
 
@@ -285,10 +291,29 @@
             tbuf.at[peer], tland.at[me % per_half], tk_s, tk_r.at[me % per_half], ep=peer
         )
 
-    @pl.when(mine)
-    def _():
-        loop(1, count, lambda t: token_copy(t).start())
-        tland[me % per_half] = tbuf[me]
+    def own_blocks(plane):
+        return pl.ds(plane * inner + side * part_spots, part_spots)
+
+    if planar:
+
+        def send_tokens(t):
+            plane = place.plane(t)
+            remote(
+                tbuf.at[own_blocks(plane)],
+                tland.at[o],
+                tk_s,
+                tk_r.at[0],
+                ep=place.at(plane, n),
+            ).start()
+
+        loop(1, outer, send_tokens)
+        tland[o] = tbuf[own_blocks(o)]
+    else:
+
+        @pl.when(mine)
+        def _():
+            loop(1, count, lambda t: token_copy(t).start())
+            tland[me % per_half] = tbuf[me]
 
     def send_route(t):
         peer = (me + t) % count
@@ -437,29 +462,18 @@
         value, outgate = value_gate[:, :size], value_gate[:, size:]
         value_columns = jnp.transpose(value)
         places = lax.broadcasted_iota(jnp.int32, (size, sequences), 1)
-        lines = lax.broadcasted_iota(jnp.int32, (sequences, size), 0)
-        across = (((1,), (1,)), ((), ()))
-
-        def some(group, readout):
-            for i in range(unroll):
-                s = group * unroll + i
-                column = jnp.where(places == s, value_columns, 0.0).astype(bf16)
-                product = jnp.dot(column, key, preferred_element_type=f32)
-                carry = carried_rows[h, pl.ds(s, 1), :]
-                write = written_rows[h, pl.ds(s, 1), :]
-                updated = carry * mem[s, h] + write * product
-                mem[s, h] = updated
-                upper = updated.astype(bf16)
-                under = (updated - upper.astype(f32)).astype(bf16)
-                answers = lax.dot_general(query, upper, across, preferred_element_type=f32)
-                answers += lax.dot_general(query, under, across, preferred_element_type=f32)
-                readout = jnp.where(lines == s, answers, readout)
-            return readout
-
-        unroll = min(sequences, 8)
-        readout = lax.fori_loop(
-            0, sequences // unroll, some, jnp.zeros((sequences, size), f32)
-        )
+        slots = lax.broadcasted_iota(jnp.int32, (size, lanes), 1)
+        query = query.astype(f32)
+        carry, write = carried_rows[h], written_rows[h]
+        answers = jnp.zeros((size, lanes), f32)
+        for s in range(sequences):
+            column = jnp.where(places == s, value_columns, 0.0).astype(bf16)
+            product = jnp.dot(column, key, preferred_element_type=f32)
+            updated = carry[s : s + 1, :] * mem[s, h] + write[s : s + 1, :] * product
+            mem[s, h] = updated
+            answer = jnp.sum(updated * query[s : s + 1, :], axis=1, keepdims=True)
+            answers = jnp.where(slots == s, answer, answers)
+        readout = jnp.transpose(answers)[:sequences]
         mean_square = jnp.mean(readout * readout, axis=-1, keepdims=True)
         gated = (
             readout
@@ -476,13 +490,14 @@
                 block, block, ag_s, ag_r.at[h], ep=place.at(place.plane(t), n)
             ).start(),
         )
-        loop(
-            1,
-            inner,
-            lambda u: remote(
-                block, block, ag_s, ap_r.at[h], ep=place.at(o, place.spot(u))
-            ).start(),
-        )
+        if not planar:
+            loop(
+                1,
+                inner,
+                lambda u: remote(
+                    block, block, ag_s, ap_r.at[h], ep=place.at(o, place.spot(u))
+                ).start(),
+            )
 
     def relay(h):
         others = gland.at[h, pl.ds(0, outer - 1)]
@@ -509,58 +524,107 @@
         def _():
             gate_math()
 
+        if planar:
+
+            @pl.when(h == heads)
+            def _():
+                loop(
+                    1,
+                    inner,
+                    lambda u: remote(
+                        mix, mixp.at[n], mx_s, mx_r, ep=place.at(o, place.spot(u))
+                    ).start(),
+                )
+
         @pl.when(h > 0)
         def _():
             memory_head(h - 1)
 
     loop(0, heads + 1, head_step)
 
-    with jax.named_scope("gated"):
-        loop(0, heads, relay)
-        partial = jnp.zeros((rows, width), f32)
-        for h in range(heads):
-            others = gland.at[h, pl.ds(0, outer * (inner - 1))]
-            remote(others, others, ag_s, ap_r.at[h], ep=me).wait_recv()
-            partial += jnp.dot(
-                gland[h].reshape(rows, size),
-                mix[h * size : (h + 1) * size, :],
-                preferred_element_type=f32,
-            )
-        partial = partial.astype(bf16)
-    pv[...] = partial.reshape(2, half, width)
-    swap = remote(pv.at[sibling], came, tp_s, tp_r, tp=sibling)
-    swap.start()
-
-    def take_tokens(b):
-        source = side * per_half + b
-
-        @pl.when(source != me)
-        def _():
-            remote(tland.at[b], tland.at[b], tk_s, tk_r.at[b], ep=source).wait_recv()
-
-    loop(0, per_half, take_tokens)
-    with jax.named_scope("swap"):
-        swap.wait_recv()
-    attended = pv[side].astype(f32) + came[...].astype(f32)
-    residual = (tland[...].reshape(half, width).astype(f32) + attended).astype(bf16)
+    def together():
+        with jax.named_scope("gated"):
+            mixp[n] = mix[...]
+            lines = []
+            for h in range(heads):
+                others = gland.at[h, pl.ds(0, outer - 1)]
+                remote(others, others, ag_s, ag_r.at[h], ep=me).wait_recv()
+                lines.append(
+                    jnp.concatenate([gland[h, place.at(a, n)] for a in range(outer)], axis=0)
+                )
+            lines = jnp.concatenate(lines, axis=1)
+            others = mixp.at[pl.ds(0, inner - 1)]
+            remote(others, others, mx_s, mx_r, ep=me).wait_recv()
+            for i in range(inner):
+                pv[i // part_spots, i % part_spots] = jnp.dot(
+                    lines, mixp[i], preferred_element_type=f32
+                ).astype(bf16)
+        swap = remote(pv.at[sibling], came, tp_s, tp_r, tp=sibling)
+        swap.start()
+        others = tland.at[pl.ds(0, outer - 1)]
+        remote(others, others, tk_s, tk_r.at[0], ep=me).wait_recv()
+        with jax.named_scope("swap"):
+            swap.wait_recv()
+        for i in range(part_spots):
+            attended = pv[side, i].astype(f32) + came[i].astype(f32)
+            base = (o * inner + side * part_spots + i) * width
+            for a in range(outer):
+                lower = a * sequences
+                res[a, n, :, pl.ds(pl.multiple_of(base, width), width)] = (
+                    tland[a, i].astype(f32) + attended[lower : lower + sequences]
+                ).astype(bf16)
+        return swap
+
+    def apart():
+        with jax.named_scope("gated"):
+            loop(0, heads, relay)
+            partial = jnp.zeros((rows, width), f32)
+            for h in range(heads):
+                others = gland.at[h, pl.ds(0, outer * (inner - 1))]
+                remote(others, others, ag_s, ap_r.at[h], ep=me).wait_recv()
+                partial += jnp.dot(
+                    gland[h].reshape(rows, size),
+                    mix[h * size : (h + 1) * size, :],
+                    preferred_element_type=f32,
+                )
+            partial = partial.astype(bf16)
+        pv[...] = partial.reshape(2, half, width)
+        swap = remote(pv.at[sibling], came, tp_s, tp_r, tp=sibling)
+        swap.start()
+
+        def take_tokens(b):
+            source = side * per_half + b
+
+            @pl.when(source != me)
+            def _():
+                remote(tland.at[b], tland.at[b], tk_s, tk_r.at[b], ep=source).wait_recv()
+
+        loop(0, per_half, take_tokens)
+        with jax.named_scope("swap"):
+            swap.wait_recv()
+        attended = pv[side].astype(f32) + came[...].astype(f32)
+        residual = (tland[...].reshape(half, width).astype(f32) + attended).astype(bf16)
+        res[me, side] = residual
+        return swap
+
+    swap = together() if planar else apart()
+
     def slot(p, core):
-        if len(res.shape) == 2:
+        if planar:
+            base = (p // inner * inner + core * part_spots) * width
             return res.at[
-                pl.ds(pl.multiple_of(core * half, half), half),
-                pl.ds(pl.multiple_of(p * width, width), width),
+                :, p % inner, :, pl.ds(pl.multiple_of(base, width), part_spots * width)
             ]
         return res.at[p, core]
 
-    slot(me, side)[...] = residual
-
     def hand(p):
         remote(slot(p, side), slot(p, side), sb_s, sb_r.at[p // inner], tp=sibling).start()
 
     def complete(t):
         plane = place.plane(t)
-        if len(res.shape) == 2:
-            across = pl.ds(pl.multiple_of(plane * inner * width, inner * width), inner * width)
-            whole = res.at[pl.ds(pl.multiple_of(sibling * half, half), half), across]
+        if planar:
+            base = (plane * inner + sibling * part_spots) * width
+            whole = res.at[:, :, :, pl.ds(pl.multiple_of(base, width), part_spots * width)]
         else:
             whole = res.at[pl.ds(plane * inner, inner), sibling]
         with jax.named_scope("settle"):
@@ -572,22 +636,33 @@
     others = rww.at[pl.ds(0, count - 1)]
     remote(others, others, rt_s, rt_r, ep=me).wait()
     with jax.named_scope("rows"):
-        gather(place, lambda p: slot(p, side), ar_s, ar_r, hand, complete)
+        gather(place, lambda p: slot(p, side), ar_s, ar_p, ar_r, hand, complete)
 
     def settle():
-        if len(res.shape) == 2:
-            rows_side = pl.ds(pl.multiple_of(side * half, half), half)
-            whole, sent = res.at[rows_side], res.at[rows_side, pl.ds(0, (count - 1) * width)]
+        if planar:
+            block = part_spots * width
+            whole = res.at[:, :, :, pl.ds(0, outer * block)]
+            sent = res.at[:, pl.ds(0, outer - 1), :, pl.ds(0, block)]
+            passed = res.at[:, pl.ds(0, inner - 1), :, pl.ds(0, outer * block)]
         else:
-            whole, sent = res.at[:, side], res.at[pl.ds(0, count - 1), side]
+            whole, sent = res.at[:, side], res.at[pl.ds(0, outer - 1), side]
+            passed = res.at[pl.ds(0, outer * (inner - 1)), side]
         remote(whole, whole, sb_s, sb_r.at[0], tp=sibling).wait_send()
         remote(sent, sent, ar_s, ar_r.at[0], ep=me).wait_send()
+        remote(passed, passed, ar_p, ar_r.at[0], ep=me).wait_send()
         others = nbuf.at[pl.ds(0, count - 1)]
         remote(others, others, p1_s, p1_r, ep=me).wait_send()
 
-        @pl.when(mine)
-        def _():
+        if planar:
+            others = tland.at[pl.ds(0, outer - 1)]
             remote(others, others, tk_s, tk_r.at[0], ep=me).wait_send()
+            others = mixp.at[pl.ds(0, inner - 1)]
+            remote(others, others, mx_s, mx_r, ep=me).wait_send()
+        else:
+
+            @pl.when(mine)
+            def _():
+                remote(others, others, tk_s, tk_r.at[0], ep=me).wait_send()
 
         others = gland1.at[pl.ds(0, inner - 1)]
         remote(others, others, g1_s, g1_r, ep=me).wait_send()
@@ -599,7 +674,7 @@
         remote(others, others, l2_s, l2_r.at[0], ep=me).wait_send()
         others = mid_half.at[:, pl.ds(0, outer - 1)]
         remote(others, others, l3_s, l3_r.at[0], ep=me).wait_send()
-        others = gland.at[:, pl.ds(0, count - 1)]
+        others = gland.at[:, pl.ds(0, (outer if planar else count) - 1)]
         remote(others, others, ag_s, ag_r.at[0], ep=me).wait_send()
         swap.wait_send()
 
@@ -659,7 +734,7 @@
     place = Place(outer, inner)
     me, side, o, n = place.me, place.side, place.o, place.n
     count = outer * inner
-    rows, model_width = res.shape
+    rows, model_width = act.shape[0], res.shape[-1]
     sequences = rows // count
     sibling = 1 - side
     hidden_chunk = wgv.shape[2]
@@ -719,7 +794,10 @@
         span = pl.ds(pl.multiple_of(plane * across, across), across)
 
         def one(r):
-            values = res[part(r), span].astype(f32)
+            if len(res.shape) == 4:
+                values = res[:, :, :, span].reshape(rows, across).astype(f32)
+            else:
+                values = res[part(r), span].astype(f32)
             squares[part(r), :] += jnp.sum(values * values, axis=-1, keepdims=True)
             scaled = (values * gain[:, span]).astype(bf16)
             for c in range(hidden_chunks):
@@ -847,10 +925,12 @@
         with jax.named_scope("sum1"):
             loop(0, chunks, first_sum)
 
-        residual = res[
-            pl.ds(pl.multiple_of(me * sequences, sequences), sequences),
-            pl.ds(pl.multiple_of(side * part_width, part_width), part_width),
-        ].astype(f32)
+        columns = pl.ds(pl.multiple_of(side * part_width, part_width), part_width)
+        if len(res.shape) == 4:
+            residual = res[o, n, :, columns].astype(f32)
+        else:
+            own_rows = pl.ds(pl.multiple_of(me * sequences, sequences), sequences)
+            residual = res[own_rows, columns].astype(f32)
 
         with jax.named_scope("sum2"):
             for c in range(chunks):
@@ -909,6 +989,7 @@
         stab_out,
         mem,
         *refs[:firsts],
+        planar=True,
         begin=begin,
         ready=arrive,
         group=group,
@@ -918,7 +999,12 @@
 
 
 def last_kernel(mixed_in, memory_in, stab_in, mixed, memory, stab, sems):
-    pairs = ((memory_in, memory), (mixed_in, mixed), (stab_in, stab))
+    parts = sems.shape[0] - 2
+    each = memory.shape[0] // parts
+    pairs = [(mixed_in, mixed), (stab_in, stab)]
+    for part in range(parts):
+        span = pl.ds(part * each, each)
+        pairs.append((memory_in.at[span], memory.at[span]))
     moves = [
         pltpu.make_async_copy(source, target, sems.at[i])
         for i, (source, target) in enumerate(pairs)
@@ -996,7 +1082,12 @@
     hidden_chunk = min(hidden, 256)
     column_chunk = min(part_width, 256)
     chunks = part_width // column_chunk
-    row_blocks = max(1, grown)
+    row_blocks = 1 if aligned else max(1, grown)
+    token_landing = (count // sides, sequences, width)
+    part_shape = (half, width)
+    if aligned:
+        token_landing = (outer, inner // sides, sequences, width)
+        part_shape = (inner // sides, outer * sequences, width)
     first_scratch = [
         pltpu.VMEM((sequences, model_width), bf16),
         pltpu.VMEM((1, model_width), f32),
@@ -1012,7 +1103,7 @@
         pltpu.VMEM((count, sequences, width), bf16),
         pltpu.VMEM((count, sequences, width), bf16),
         pltpu.VMEM((count, sequences, width), bf16),
-        pltpu.VMEM((count // sides, sequences, width), bf16),
+        pltpu.VMEM(token_landing, bf16),
         pltpu.VMEM((count, 1, lanes), f32),
         pltpu.VMEM((outer, inner, sequences, lanes), bf16),
         pltpu.VMEM((inner, outer, sequences, lanes), bf16),
@@ -1028,13 +1119,14 @@
         pltpu.VMEM((heads, sequences, lanes), f32),
         pltpu.VMEM((heads, sequences, lanes), f32),
         pltpu.VMEM((heads, count, sequences, size), bf16),
-        pltpu.VMEM((sides, half, width), bf16),
-        pltpu.VMEM((half, width), bf16),
+        pltpu.VMEM((sides,) + part_shape, bf16),
+        pltpu.VMEM(part_shape, bf16),
+        pltpu.VMEM((inner, head_width, width), bf16),
     ]
     first_scratch += copies(10, 4 * heads)
     first_scratch += copies(0, 0, 0, count // sides, 0, 0, 0, 0, 0, 0)
     first_scratch += copies(0, heads * outer, 0, heads, 0, heads, heads)
-    first_scratch += copies(0, heads, heads, 0, 0, 0, count, 0, outer)
+    first_scratch += copies(0, heads, heads, 0, 0, 0, count, 0, outer, 0, 0, 0)
     second_scratch = [
         pltpu.VMEM((1, model_width), f32),
         pltpu.VMEM((1, model_width), f32),
@@ -1101,7 +1193,7 @@
             in_specs=[in_place()] * 23,
             out_specs=(in_vmem(),) * 3,
             scratch_shapes=[
-                pltpu.VMEM((rows, model_width), bf16),
+                pltpu.VMEM((outer, inner, sequences, model_width), bf16),
                 pltpu.VMEM((count, 1, lanes), f32),
             ]
             + first_scratch
@@ -1146,7 +1238,7 @@
         ),
         in_specs=[in_vmem()] * 3,
         out_specs=(in_place(),) * 3,
-        scratch_shapes=copies(3),
+        scratch_shapes=copies(2 + min(sequences, 8)),
         compiler_params=pltpu.CompilerParams(vmem_limit_bytes=8 * 2**20),
     )(mixed, memory_new, stab_new)
     return (mixed, memory_new, stab_new.T)

time: 67.7 us -> 62.4 us (0.922)
  Pallas kernels: 66.9 us -> 61.6 us
    pallas_call x1, Pallas kernels: 64.9 us -> 59.5 us  [body(): pl.pallas_call(functools.partial(whole_kernel, outer, inner, chunks, row_...]
where the time goes in v3:
time: 62.4 us; the launch traced here: 62.3 us
  Pallas kernels  61.6 us (99%)
  between operations  0.65 us (1%)
    pallas_call x1, Pallas kernels, body(): pl.pallas_call(functools.partial(whole_kernel, outer, inner, chunks, row_...  59.5 us
    pallas_call x1, Pallas kernels, body(): pl.pallas_call(last_kernel, out_shape=tuple((jax.ShapeDtypeStruct(array.s...  2.1 us

profile of v3, /device:TPU:0, one launch (start us, length us, event | category | flops | bytes accessed | tf_op | source)
XLA Modules:
  0.0 62.3 jit_solution(12870494054912782449)
XLA Ops:
  0.6 59.5 %shard_map.238 = (bf16[16,1024]{1,0:T(8,128)(2,1)S(1)}, f32[4,16]{1,0:T(4,128)S(1)}, f32[16,4,128,128]{3,2,1,0:T(8,128)S(1)}) custom-call(bf16[16,2048]{1,0:T(8,128)(2,1)} %refs_0_.1, f32[1,2048]{1,0:T(1,128)} %bitcast.11, bf16[128,512]{1,0:T(8,128)(2,1)} %refs_2_.1, bf16[128,512]{1,0:T(8,128)(2,1)} %refs_3_.1, bf16[128,512]{1,0:T(8,128)(2,1)} %refs_4_.1, ...), custom_call_target="tpu_custom_call" | custom-call | tf_op jit(solution)/shard_map/pallas_call | solution.py:1188
  60.1 2.1 %shard_map.239 = (bf16[16,1024]{1,0:T(8,128)(2,1)}, f32[16,4,128,128]{3,2,1,0:T(8,128)}, f32[4,16]{1,0:T(4,128)}) custom-call(bf16[16,1024]{1,0:T(8,128)(2,1)S(1)} %get-tuple-element.9.mixed_in, f32[16,4,128,128]{3,2,1,0:T(8,128)S(1)} %get-tuple-element.10.memory_in, f32[4,16]{1,0:T(4,128)S(1)} %get-tuple-element.11.stab_in), custom_call_target="tpu_custom_call" | custom-call | tf_op jit(solution)/shard_map/pallas_call | solution.py:1233

commit v4 on v3

--- a/solution.py
+++ b/solution.py
@@ -49,7 +49,8 @@
         self.n = self.me % inner
 
     def plane(self, step):
-        return (self.o + step) % self.outer
+        turn = 1 - 2 * (2 * self.o // self.outer)
+        return (self.o + turn * step + self.outer) % self.outer
 
     def spot(self, step):
         return (self.n + step) % self.inner

time: 62.4 us -> 61.9 us (level)
  no operation moved by 1% of the time
where the time goes in v4:
time: 61.9 us; the launch traced here: 61.8 us
  Pallas kernels  61.1 us (99%)
  between operations  0.65 us (1%)
    pallas_call x1, Pallas kernels, body(): pl.pallas_call(functools.partial(whole_kernel, outer, inner, chunks, row_...  59 us
    pallas_call x1, Pallas kernels, body(): pl.pallas_call(last_kernel, out_shape=tuple((jax.ShapeDtypeStruct(array.s...  2.1 us

profile of v4, /device:TPU:0, one launch (start us, length us, event | category | flops | bytes accessed | tf_op | source)
XLA Modules:
  0.0 61.8 jit_solution(4526555665296312876)
XLA Ops:
  0.6 59.0 %shard_map.238 = (bf16[16,1024]{1,0:T(8,128)(2,1)S(1)}, f32[4,16]{1,0:T(4,128)S(1)}, f32[16,4,128,128]{3,2,1,0:T(8,128)S(1)}) custom-call(bf16[16,2048]{1,0:T(8,128)(2,1)} %refs_0_.1, f32[1,2048]{1,0:T(1,128)} %bitcast.11, bf16[128,512]{1,0:T(8,128)(2,1)} %refs_2_.1, bf16[128,512]{1,0:T(8,128)(2,1)} %refs_3_.1, bf16[128,512]{1,0:T(8,128)(2,1)} %refs_4_.1, ...), custom_call_target="tpu_custom_call" | custom-call | tf_op jit(solution)/shard_map/pallas_call | solution.py:1189
  59.6 2.1 %shard_map.239 = (bf16[16,1024]{1,0:T(8,128)(2,1)}, f32[16,4,128,128]{3,2,1,0:T(8,128)}, f32[4,16]{1,0:T(4,128)}) custom-call(bf16[16,1024]{1,0:T(8,128)(2,1)S(1)} %get-tuple-element.9.mixed_in, f32[16,4,128,128]{3,2,1,0:T(8,128)S(1)} %get-tuple-element.10.memory_in, f32[4,16]{1,0:T(4,128)S(1)} %get-tuple-element.11.stab_in), custom_call_target="tpu_custom_call" | custom-call | tf_op jit(solution)/shard_map/pallas_call | solution.py:1234
